TPU v7x, 128 devices: a whole 4x4x4 slice. The times are simulated.
128 devices in a mesh: sp: 32 (over z, y, core), tp: 4 (over x).
Axes of the slice: x: 4, y: 4, z: 4, core: 2. Of those that a mesh axis runs over, the one named last changes fastest.
Arguments:
- queries: bfloat16 [24576, 1024], P('sp', 'tp'), may hold values from -6 to 6
- keys: bfloat16 [24576, 1024], P('sp', 'tp'), may hold values from -6 to 6
- values: bfloat16 [24576, 2048], P('sp', 'tp'), may hold values from -6 to 6
- out_gate: bfloat16 [24576, 2048], P('sp', 'tp'), may hold values from -6 to 6
- input_gates: float32 [2, 4, 24576], P(None, 'tp', 'sp'), may hold values from -4 to 300
- forget_gates: float32 [2, 4, 24576], P(None, 'tp', 'sp'), may hold values from -1 to 16
- doc_ids: int32 [24576], P('sp'), may hold values from 0 to 15, never falling along the last dimension, each value on 1 to 3072 neighbouring positions
- head_gain: float32 [2048], P('tp'), may hold values from 0.1 to 1.9
- w_out: bfloat16 [2048, 2048], P('tp'), may hold values from -0.25 to 0.25
- resid: bfloat16 [24576, 2048], P(('sp', 'tp')), may hold values from -30 to 30
- norm_gain: float32 [2048], replicated, may hold values from 0.1 to 1.9
- w_up: bfloat16 [2048, 8192], P('sp', 'tp'), may hold values from -0.125 to 0.125
- w_down: bfloat16 [8192, 2048], P('tp', 'sp'), may hold values from -0.0625 to 0.0625
Outputs:
- layer_out: bfloat16 [24576, 2048], P(('sp', 'tp'))
Inputs may be any that keep to these rules, and one draw needn't show every extreme that they name: `doc_ids`: document numbers never fall along the positions.
All inputs are finite; a program needn't handle non-finite values.
Results may differ from a plain program's by a relative error of at most 0.013.
Values may be sent and summed in bfloat16 or wider, within the bound.
A program may use at most 128 MiB of HBM per device.

v0:
```python
import jax
import jax.numpy as jnp
from jax import lax
from jax.sharding import Mesh
from jax.sharding import PartitionSpec as P

SP = ("sp_0", "sp_1", "sp_2")
SP_TP = ("sp_0", "sp_1", "sp_2", "tp")


eps = 1e-06
far_low = -1e30


def neutral_like(value, identity):
    return jax.tree.map(
        lambda a, e: jnp.broadcast_to(jnp.asarray(e, a.dtype), a.shape), value, identity
    )


def gathered_once(value, axis):
    leaves = jax.tree.leaves(value)
    turns = sorted(range(len(leaves)), key=lambda k: -leaves[k].size)
    width = (1, *leaves[turns[0]].shape)[-1]
    lines = [
        jnp.pad(leaves[k].reshape(-1), (0, -leaves[k].size % width)).reshape(-1, width)
        for k in turns
    ]
    both, at, found = (lax.all_gather(jnp.concatenate(lines), axis), 0, {})
    for k, line in zip(turns, lines):
        section = both[:, at : at + len(line)].reshape(len(both), -1)
        found[k] = section[:, : leaves[k].size].reshape(-1, *leaves[k].shape)
        at += len(line)
    numbers = iter(range(len(leaves)))
    return jax.tree.map(lambda _: found[next(numbers)], value)


def carried_in(value, axes, combine, identity, reverse):
    before = start = neutral_like(value, identity)
    running = value
    for axis in reversed(axes):
        length, index = (lax.axis_size(axis), lax.axis_index(axis))
        pieces = gathered_once(
            jax.tree.map(
                lambda part, kind: part.astype(kind),
                running,
                jax.tree.map(lambda a: jnp.bfloat16 if a.dtype == jnp.float32 else a.dtype, value),
            ),
            axis,
        )
        inside, running = (start, start)
        for k in reversed(range(length)) if reverse else range(length):
            passed = k > index if reverse else k < index
            running = combine(
                running, jax.tree.map(lambda part, own: part[k].astype(own.dtype), pieces, value)
            )
            inside = jax.tree.map(lambda new, old: jnp.where(passed, new, old), running, inside)
        before = combine(inside, before)
    return before


def split_up(value, dim, length):
    dims = value.shape
    pieces = value.reshape(*dims[:dim], length, dims[dim] // length, *dims[dim + 1 :])
    return jnp.moveaxis(pieces, dim, 0)


def sent_and_summed(value, axis, dim):
    length = lax.axis_size(axis)
    pieces = lax.all_to_all(split_up(value, dim, length), axis, 0, 0, tiled=True)
    return jnp.sum(pieces.astype(jnp.float32), axis=0)


def summarize(keys_blk, values_blk, in_gate, forget_pre, doc_pos):
    logf = jax.nn.log_sigmoid(forget_pre)
    cum = jnp.cumsum(logf)
    length = keys_blk.shape[0]
    last_doc = doc_pos[length - 1]
    tail = doc_pos == last_doc
    total = cum[length - 1]
    exponent = jnp.where(tail, total - cum + in_gate, far_low)
    peak = jnp.max(exponent)
    scaled = jnp.exp(exponent - peak)
    weighted = (keys_blk * scaled[:, None]).astype(jnp.bfloat16)
    memory = jnp.einsum("sd,sv->dv", weighted, values_blk, preferred_element_type=jnp.float32)
    norm_keys = jnp.sum(weighted.astype(jnp.float32), axis=0)
    return (memory, norm_keys, peak, total, doc_pos[0], last_doc, jnp.zeros((), jnp.float32))


def emit(queries_blk, keys_blk, values_blk, in_gate, forget_pre, doc_pos, state):
    memory, norm_keys, top_in, total_in, first_in, last_in, empty_in = state
    scale = queries_blk.shape[1] ** (-0.5)
    logf = jax.nn.log_sigmoid(forget_pre)
    cum = jnp.cumsum(logf)
    length = queries_blk.shape[0]
    place = jnp.arange(length)
    keep = (place[:, None] >= place[None, :]) & (doc_pos[:, None] == doc_pos[None, :])
    exponent = jnp.where(keep, cum[:, None] - cum[None, :] + in_gate[None, :], far_low)
    usable = (doc_pos == last_in) & (empty_in < 0.5)
    carried = jnp.where(usable, cum + top_in, far_low)
    peak = jnp.maximum(carried, jnp.max(exponent, axis=1))
    scores = (
        jnp.einsum("td,sd->ts", queries_blk, keys_blk, preferred_element_type=jnp.float32) * scale
    )
    weights = jnp.where(keep, scores * jnp.exp(exponent - peak[:, None]), 0.0)
    inter = jnp.where(usable, jnp.exp(carried - peak), 0.0)
    query_wide = queries_blk.astype(jnp.float32)
    numer = jnp.dot(weights.astype(jnp.bfloat16), values_blk, preferred_element_type=jnp.float32)
    numer = numer + (inter * scale)[:, None] * jnp.dot(query_wide, memory)
    denom = jnp.sum(weights, axis=1) + inter * scale * jnp.dot(query_wide, norm_keys)
    return numer / jnp.maximum(jnp.abs(denom), 1.0)[:, None]


def combine(early, late):
    e_mem, e_keys, e_top, e_total, e_first, e_last, e_empty = early
    l_mem, l_keys, l_top, l_total, l_first, l_last, l_empty = late
    linked = (l_first == e_last) & (l_first == l_last) & (e_empty < 0.5)
    top = jnp.where(linked, jnp.maximum(l_top, e_top + l_total), l_top)
    early_part = jnp.where(linked, jnp.exp(jnp.minimum(e_top + l_total - top, 0.0)), 0.0)
    late_part = jnp.exp(l_top - top)
    joined = (
        early_part * e_mem + late_part * l_mem,
        early_part * e_keys + late_part * l_keys,
        top,
        e_total + l_total,
        jnp.where(e_empty > 0.5, l_first, e_first),
        l_last,
        jnp.zeros_like(l_empty),
    )
    return tuple((jnp.where(l_empty > 0.5, a, b) for a, b in zip(early, joined)))


def direction(queries3, keys3, values3, in_gates, forget_pre, doc_pos, backward):
    if backward:
        queries3, keys3, values3 = (queries3[::-1], keys3[::-1], values3[::-1])
        in_gates, forget_pre, doc_pos = (in_gates[:, ::-1], forget_pre[:, ::-1], doc_pos[::-1])
    summary = jax.vmap(summarize, in_axes=(1, 1, 0, 0, None))(
        keys3, values3, in_gates, forget_pre, doc_pos
    )
    heads = in_gates.shape[0]
    start = (
        jnp.zeros((heads, keys3.shape[2], values3.shape[2]), jnp.float32),
        jnp.zeros((heads, keys3.shape[2]), jnp.float32),
        jnp.full((heads,), far_low, jnp.float32),
        jnp.zeros((heads,), jnp.float32),
        jnp.full((heads,), -1.0, jnp.float32),
        jnp.full((heads,), -1.0, jnp.float32),
        jnp.ones((heads,), jnp.float32),
    )
    if backward:
        incoming = carried_in(summary, SP, jax.vmap(combine), start, True)
    else:
        incoming = carried_in(summary, SP, jax.vmap(combine), start, False)
    result = jax.vmap(emit, in_axes=(1, 1, 1, 0, 0, None, 0), out_axes=1)(
        queries3, keys3, values3, in_gates, forget_pre, doc_pos, incoming
    )
    if backward:
        result = result[::-1]
    return result


def fetch_weights(w_up, w_down):
    up_full = lax.all_gather(w_up, SP, axis=0, tiled=True)
    down_full = lax.all_gather(w_down, SP, axis=1, tiled=True)
    return (up_full, down_full)


def rms_scale(mixed, norm_gain):
    factor = lax.rsqrt(jnp.mean(mixed * mixed, axis=-1, keepdims=True) + eps)
    return (mixed * factor * norm_gain).astype(jnp.bfloat16)


def shards(
    queries,
    keys,
    values,
    out_gate,
    input_gates,
    forget_gates,
    doc_ids,
    head_gain,
    w_out,
    resid,
    norm_gain,
    w_up,
    w_down,
):
    length = queries.shape[0]
    heads = input_gates.shape[1]
    queries3 = queries.reshape(length, heads, -1)
    keys3 = keys.reshape(length, heads, -1)
    values3 = values.reshape(length, heads, -1)
    doc_pos = doc_ids.astype(jnp.float32)
    memory = direction(queries3, keys3, values3, input_gates[0], forget_gates[0], doc_pos, False)
    memory = memory + direction(
        queries3, keys3, values3, input_gates[1], forget_gates[1], doc_pos, True
    )
    normed = memory * lax.rsqrt(jnp.mean(memory * memory, axis=-1, keepdims=True) + eps)
    gate = jax.nn.sigmoid(out_gate.astype(jnp.float32)).reshape(length, heads, -1)
    readout = (
        (normed * head_gain.reshape(heads, -1) * gate).astype(jnp.bfloat16).reshape(length, -1)
    )
    up_full, down_full = fetch_weights(w_up, w_down)
    picked = readout
    mixed = resid.astype(jnp.float32) + sent_and_summed(
        jnp.dot(picked, w_out, preferred_element_type=jnp.float32).astype(jnp.bfloat16), "tp", 0
    )
    scaled = rms_scale(mixed, norm_gain)
    product = jnp.dot(
        lax.all_gather(scaled, "tp", axis=0, tiled=True),
        up_full,
        preferred_element_type=jnp.float32,
    )
    hidden = jnp.square(jax.nn.relu(product)).astype(jnp.bfloat16)
    picked = hidden
    return (
        mixed
        + sent_and_summed(
            jnp.dot(picked, down_full, preferred_element_type=jnp.float32).astype(jnp.bfloat16),
            "tp",
            0,
        )
    ).astype(jnp.bfloat16)


def solution(mesh):
    split = Mesh(mesh.devices.reshape(4, 4, 2, mesh.shape["tp"]), ("sp_0", "sp_1", "sp_2", "tp"))
    return jax.shard_map(
        shards,
        mesh=split,
        in_specs=(
            P(SP, "tp"),
            P(SP, "tp"),
            P(SP, "tp"),
            P(SP, "tp"),
            P(None, "tp", SP),
            P(None, "tp", SP),
            P(SP),
            P("tp"),
            P("tp", None),
            P(SP_TP, None),
            P(),
            P(SP, "tp"),
            P("tp", SP),
        ),
        out_specs=P(SP_TP, None),
        check_vma=False,
    )
```

profile of v0, /device:TPU:0, one launch (start us, length us, event | category | flops | bytes accessed | tf_op | source)
XLA Modules:
  0.0 496.2 jit_solution(1414788614506800733)
XLA Ops:
  13.3 2.1 fusion.304
  17.8 1.9 convolution_convert_fusion.3
  20.6 2.2 all-gather.6
  37.3 1.4 concatenate.19
  38.8 3.8 reverse.15
  42.7 11.9 %reverse.16 = bf16[768,512]{1,0:T(8,128)(2,1)} reverse(bf16[768,512]{1,0:T(8,128)(2,1)} %param.15), dimensions={0} | reverse | bytes 1572864 | tf_op jit(solution)/shard_map/reverse.3
  58.3 1.3 fusion.305
  60.9 1.2 fusion.205
  62.0 1.8 convolution_convert_fusion.2
  64.1 2.2 all-gather.9
  80.7 1.4 concatenate.22
  111.6 1.5 fusion.146
  113.1 1.4 concatenate.20
  144.4 1.5 fusion.147
  145.9 1.4 concatenate.23
  147.7 6.3 %reverse.14 = bf16[768,256]{1,0:T(8,128)(2,1)} reverse(bf16[768,256]{1,0:T(8,128)(2,1)} %param.13), dimensions={0} | reverse | bytes 786432 | tf_op jit(solution)/shard_map/reverse
  154.0 2.3 copy.540
  206.5 2.1 fusion.344
  208.6 2.0 fusion.9
  211.5 1.5 fusion.343
  214.2 4.4 fusion.4
  218.5 13.6 %reverse.17 = f32[768,512]{0,1:T(8,128)} reverse(f32[768,512]{0,1:T(8,128)} %fusion.4), dimensions={0} | reverse | bytes 3145728 | tf_op jit(solution)/shard_map/reverse.5
  232.4 4.4 multiply_reduce_fusion.1
  236.8 2.0 convolution_convert_fusion.1
  238.8 42.3 %all_to_all.10 = bf16[4,192,2048]{2,1,0:T(8,128)(2,1)S(1)} all-to-all(bf16[4,192,2048]{2,1,0:T(8,128)(2,1)S(1)} %bitcast.464), channel_id=1, replica_groups=mesh['sp_0'=4,'sp_1'=4,'sp_2'=2,'tp'=4] {'tp'}, dimensions={0} | all-to-all | bytes 6291456 | tf_op jit(solution)/shard_map/all_to_all | solution.py:70
  285.8 38.8 %all-gather.20.cloned.1.call-done = bf16[768,2048]{1,0:T(8,128)(2,1)} async-done(((bf16[192,2048]{1,0:T(8,128)(2,1)}), bf16[768,2048]{1,0:T(8,128)(2,1)}) %all-gather.20.cloned.1.call-update) | async-done | bytes 3145744 | tf_op jit(solution)/shard_map/all_gather | solution.py:210
  324.7 55.2 %all-gather.22.cloned.1.call-done = bf16[2048,2048]{1,0:T(8,128)(2,1)} async-done(((bf16[64,2048]{1,0:T(8,128)(2,1)}), bf16[2048,2048]{1,0:T(8,128)(2,1)}) %all-gather.22.cloned.1.call-update) | async-done | bytes 8388624 | tf_op jit(solution)/shard_map/all_gather | solution.py:163
  379.9 11.9 %multiply_convert_fusion = bf16[768,2048]{1,0:T(8,128)(2,1)} fusion(bf16[768,2048]{1,0:T(8,128)(2,1)} %all-gather.20.cloned.1.call-done, bf16[2048,2048]{1,0:T(8,128)(2,1)} %all-gather.22.cloned.1.call-done), kind=kOutput, calls=%fused_computation.1 | convolution fusion | flops 6447169536 | bytes 14680064 | tf_op jit(solution)/shard_map/dot_general | solution.py:209
  391.8 42.8 %all-gather.24.cloned.1.call-done = bf16[2048,2048]{0,1:T(8,128)(2,1)} async-done(((bf16[2048,64]{0,1:T(8,128)(2,1)}), bf16[2048,2048]{0,1:T(8,128)(2,1)}) %all-gather.24.cloned.1.call-update) | async-done | bytes 8388624 | tf_op jit(solution)/shard_map/all_gather | solution.py:164
  434.5 10.1 %convolution_convert_fusion = bf16[768,2048]{1,0:T(8,128)(2,1)S(1)} fusion(bf16[768,2048]{1,0:T(8,128)(2,1)} %multiply_convert_fusion, bf16[2048,2048]{0,1:T(8,128)(2,1)} %all-gather.24.cloned.1.call-done), kind=kOutput, calls=%fused_computation.3 | convolution fusion | flops 6444023808 | bytes 14680064 | tf_op jit(solution)/shard_map/dot_general | solution.py:219
  444.6 42.0 %all_to_all.11 = bf16[4,192,2048]{2,1,0:T(8,128)(2,1)S(1)} all-to-all(bf16[4,192,2048]{2,1,0:T(8,128)(2,1)S(1)} %bitcast.465), channel_id=1, replica_groups=mesh['sp_0'=4,'sp_1'=4,'sp_2'=2,'tp'=4] {'tp'}, dimensions={0} | all-to-all | bytes 6291456 | tf_op jit(solution)/shard_map/all_to_all | solution.py:70
  488.1 1.2 add_convert_fusion
  (232 shorter events, 42.6 us)
Async XLA Ops:
  6.5 230.3 %copy-start = (bf16[512,2048]{1,0:T(8,128)(2,1)S(1)}, bf16[512,2048]{1,0:T(8,128)(2,1)}, u32[]{:S(2)}) copy-start(bf16[512,2048]{1,0:T(8,128)(2,1)} %param.21) | copy-start | bytes 6291460
  6.5 75.6 %all-gather.26.cloned.1.call-start = ((), (), s32[]{:S(2)}) async-start(), calls=%async_computation.5 | async-start | bytes 1351680 | tf_op jit(solution)/shard_map/all_gather | solution.py:29
  17.8 21.0 %copy-start.5 = (bf16[768,256]{1,0:T(8,128)(2,1)S(1)}, bf16[768,256]{1,0:T(8,128)(2,1)}, u32[]{:S(2)}) copy-start(bf16[768,256]{1,0:T(8,128)(2,1)} %param.14) | copy-start | bytes 1179652
  38.7 75.9 %all-gather.30.cloned.1.call-start = ((), (), s32[]{:S(2)}) async-start(), calls=%async_computation.7 | async-start | bytes 1351680 | tf_op jit(solution)/shard_map/all_gather | solution.py:29
  82.1 75.9 %all-gather.28.cloned.1.call-start = ((), (), s32[]{:S(2)}) async-start(), calls=%async_computation.6 | async-start | bytes 1351680 | tf_op jit(solution)/shard_map/all_gather | solution.py:29
  114.5 67.6 %all-gather.32.cloned.1.call-start = ((), (), s32[]{:S(2)}) async-start(), calls=%async_computation.8 | async-start | bytes 1351680 | tf_op jit(solution)/shard_map/all_gather | solution.py:29
  145.9 60.5 %copy-start.12 = (s32[768]{0:T(1024)S(1)}, s32[768]{0:T(1024)}, u32[]{:S(2)}) copy-start(s32[768]{0:T(1024)} %param.19) | copy-start | bytes 9220
  147.3 177.3 %all-gather.20.cloned.1.call-start = ((), (), s32[]{:S(2)}) async-start(), calls=%async_computation.2 | async-start | bytes 3932160 | tf_op jit(solution)/shard_map/all_gather | solution.py:210
  206.5 2.1 copy-start.9
  208.6 2.9 copy-start.7
  208.6 2.9 copy-start.8
  211.5 1.5 copy-start.10
  218.5 13.6 %copy-start.6 = (bf16[768,256]{1,0:T(8,128)(2,1)S(1)}, bf16[768,256]{1,0:T(8,128)(2,1)}, u32[]{:S(2)}) copy-start(bf16[768,256]{1,0:T(8,128)(2,1)} %param.13) | copy-start | bytes 1179652
  232.4 4.4 copy-start.11
  232.4 4.4 copy-start.14
  281.1 1.1 copy-start.4
  282.2 1.1 copy-start.2
  282.2 1.1 copy-start.13
  284.5 95.4 %all-gather.22.cloned.1.call-start = ((), (), s32[]{:S(2)}) async-start(), calls=%async_computation.3 | async-start | bytes 8650752 | tf_op jit(solution)/shard_map/all_gather | solution.py:163
  285.1 149.5 %all-gather.24.cloned.1.call-start = ((), (), s32[]{:S(2)}) async-start(), calls=%async_computation.4 | async-start | bytes 8650752 | tf_op jit(solution)/shard_map/all_gather | solution.py:164
  486.7 1.4 copy-start.3
  486.7 2.6 copy-start.1
Sparse Core Ops, SparseCore 0:
  38.8 26.7 all-gather.25
  82.2 26.6 all-gather.29
  114.6 26.8 all-gather.27
  147.5 26.8 all-gather.31
  284.6 39.9 all-gather.19
  326.8 53.0 all-gather.21
  382.1 52.3 all-gather.23
where the time goes:
time: 502 us; the launch traced here: 496 us
  waiting for transfers between devices  138 us (27%)
  between operations  134 us (27%)
  blocking collectives  88.7 us (18%)
  local copies, waits for them, and re-layouts  72.9 us (15%)
  matrix products  43.3 us (9%)
  other arithmetic  18.8 us (4%)
    all_to_all x2, blocking collectives, sent_and_summed(): lax.all_to_all(split_up(value, dim, length), axis, 0, 0, tiled=True)  84.3 us
    all_gather x1, waiting for transfers between devices, fetch_weights(): up_full = lax.all_gather(w_up, SP, axis=0, tiled=True)  55.2 us
    all_gather x1, waiting for transfers between devices, fetch_weights(): down_full = lax.all_gather(w_down, SP, axis=1, tiled=True)  42.8 us
    all_gather x1, waiting for transfers between devices, shards(): lax.all_gather(scaled, 'tp', axis=0, tiled=True)  38.8 us
    another operation x7, local copies, waits for them, and re-layouts  35.8 us
    slice x30, local copies, waits for them, and re-layouts, carried_in(): part[k].astype(own.dtype)  17.1 us
    dot_general x1, matrix products, shards(): jnp.dot(lax.all_gather(scaled, 'tp', axis=0, tiled=True), up_full, prefer...  11.9 us
    dot_general x1, matrix products, shards(): jnp.dot(picked, down_full, preferred_element_type=jnp.float32)  10.1 us
  transfers between devices with their start and end apart: 7, of which 3 were waited for; matrix products, arithmetic and copies ran while one was open for 14% of the time, Pallas kernels for 0%

commit v1 on v0

v1 whole, which is shorter than its diff:
```python
import functools

import jax
import jax.numpy as jnp
from jax import lax
from jax.experimental import pallas as pl
from jax.experimental.pallas import tpu as pltpu
from jax.sharding import Mesh
from jax.sharding import PartitionSpec as P

MESH = pl.DeviceIdType.MESH
F32 = jnp.float32
BF16 = jnp.bfloat16
EPS = 1e-06
FAR_LOW = -1e30

T = 768
ROWS = 192
HALF = 96
DK = 256
DV = 512
D = 2048
SROWS = 272
SCALE = DK ** (-0.5)
N_SEMS = 96


class Copies:
    def __init__(self, send, recv, loc):
        self.send, self.recv, self.loc = send, recv, loc
        self.at = 0
        self.at_loc = 0
        self.all = []

    def remote(self, src, dst, dev):
        k = self.at
        self.at += 1
        assert k < N_SEMS
        c = pltpu.make_async_remote_copy(
            src_ref=src,
            dst_ref=dst,
            send_sem=self.send.at[k],
            recv_sem=self.recv.at[k],
            device_id=dev,
            device_id_type=MESH,
        )
        self.all.append(c)
        return c

    def local(self, src, dst):
        k = self.at_loc
        self.at_loc += 1
        return pltpu.make_async_copy(src, dst, self.loc.at[k])


class Ring:
    def __init__(self, cp, plus, minus, own, put_plus, put_minus, near0, near1, far0, far1):
        self.p0 = cp.remote(own(0), put_plus(0), plus)
        self.m0 = cp.remote(own(1), put_minus(1), minus)
        self.p1 = cp.remote(own(1), put_plus(1), plus)
        self.m1 = cp.remote(own(0), put_minus(0), minus)
        self.rp = cp.remote(near0, far0, plus)
        self.rm = cp.remote(near1, far1, minus)

    def start(self):
        for c in (self.p0, self.m0, self.p1, self.m1):
            c.start()

    def relay(self):
        self.p0.wait_recv()
        self.rp.start()
        self.m0.wait_recv()
        self.rm.start()

    def near(self):
        self.p1.wait_recv()
        self.m1.wait_recv()

    def far(self):
        self.rp.wait_recv()
        self.rm.wait_recv()


def slot_ring(cp, axis, p, slot):
    plus, minus = lax.rem(p + 1, 4), lax.rem(p + 3, 4)
    own = lambda h: slot(p, h)
    return Ring(
        cp, {axis: plus}, {axis: minus}, own, own, own,
        slot(minus, 0), slot(plus, 1), slot(minus, 0), slot(plus, 1),
    )


def roll_lanes(x, shift):
    return pltpu.roll(x, shift % T, 1)


def kernel(
    ig_ref, fg_ref, doc_ref, gain_ref, ngain_ref,
    q_h, k_h, v_h, og_h, wout_h, resid_h, wup_h, wdn_h,
    out_ref,
    wu, wd, wo, wa, wb, q, k, v, og, resid,
    arow, cols, numf, numb, dens,
    st_own, st_par, sc_pair, q_send, q_recv, sc_recv, cin,
    ro_out, ro, mixed, nrm, hid, part, acc2, add_in, rs_in,
    send_sem, recv_sem, loc_sem,
):
    z, y, c, x = (lax.axis_index(a) for a in ("z", "y", "c", "x"))
    other = 1 - c
    n = z * 4 + y
    n_up, n_dn = lax.rem(n + 1, 16), lax.rem(n + 15, 16)
    chip_up = {"z": lax.div(n_up, 4), "y": lax.rem(n_up, 4)}
    chip_dn = {"z": lax.div(n_dn, 4), "y": lax.rem(n_dn, 4)}
    partner = {"c": other}
    xp, xm, xf = lax.rem(x + 1, 4), lax.rem(x + 3, 4), lax.rem(x + 2, 4)
    cp = Copies(send_sem, recv_sem, loc_sem)

    l_wd = cp.local(wdn_h, wa)
    l_wu = cp.local(wup_h, wu.at[z, y, c])
    l_k = cp.local(k_h, k)
    l_v = cp.local(v_h, v)
    l_q = cp.local(q_h, q)
    l_wo = [cp.local(wout_h.at[pl.ds(256 * i, 256)], wo.at[x, i]) for i in range(2)]
    l_og = cp.local(og_h, og)
    l_re = cp.local(resid_h, resid)
    for l in (l_wd, l_wu, l_k, l_v, l_q, *l_wo, l_og, l_re):
        l.start()

    barrier = pltpu.get_barrier_semaphore()
    peers = (
        partner, {"y": lax.rem(y + 1, 4)}, {"y": lax.rem(y + 3, 4)}, {"z": lax.rem(z + 1, 4)},
        {"z": lax.rem(z + 3, 4)}, {"x": xp}, {"x": xm}, {"x": xf}, chip_up, chip_dn,
    )
    for dev in peers:
        pl.semaphore_signal(barrier, inc=1, device_id=dev, device_id_type=MESH)
    pl.semaphore_wait(barrier, len(peers))

    a1 = slot_ring(cp, "y", y, lambda p, h: wu.at[z, p, c, pl.ds(32 * h, 32)])
    a2 = slot_ring(cp, "z", z, lambda p, h: wu.at[p, :, c, pl.ds(32 * h, 32)])
    b1 = slot_ring(cp, "z", z, lambda p, h: wd.at[p, y, c, pl.ds(512 * h, 512)])
    b2 = slot_ring(cp, "y", y, lambda p, h: wd.at[:, p, c, pl.ds(512 * h, 512)])
    wr = slot_ring(cp, "x", x, lambda p, h: wo.at[p, c, pl.ds(128 * h, 128)])

    l_wd.wait()
    d_wd = cp.remote(wa.at[pl.ds(pl.multiple_of(1024 * other, 1024), 1024)], wb, partner)
    d_wd.start()
    l_wu.wait()
    a1.start()
    for l in l_wo:
        l.wait()
    wr.start()

    def row(ref, i):
        return jnp.broadcast_to(ref[i], (8, T))

    lane = lax.broadcasted_iota(jnp.int32, (8, T), 1)
    rowi = lax.broadcasted_iota(jnp.int32, (8, T), 0)
    doc = jnp.broadcast_to(doc_ref[...], (8, T)).astype(F32)

    def log_sigmoid(f):
        return jnp.minimum(f, 0.0) - jnp.log1p(jnp.exp(-jnp.abs(f)))

    cumf, cumb = log_sigmoid(row(fg_ref, 0)), log_sigmoid(row(fg_ref, 1))
    sh = 1
    while sh < T:
        cumf = cumf + jnp.where(lane >= sh, roll_lanes(cumf, sh), 0.0)
        cumb = cumb + jnp.where(lane < T - sh, roll_lanes(cumb, T - sh), 0.0)
        sh *= 2
    af, ab = row(ig_ref, 0) - cumf, row(ig_ref, 1) - cumb
    mf, mb = af, ab
    sh = 1
    while sh < T:
        same_f = (lane >= sh) & (roll_lanes(doc, sh) == doc)
        same_b = (lane < T - sh) & (roll_lanes(doc, T - sh) == doc)
        mf = jnp.where(same_f, jnp.maximum(mf, roll_lanes(mf, sh)), mf)
        mb = jnp.where(same_b, jnp.maximum(mb, roll_lanes(mb, T - sh)), mb)
        sh *= 2
    doc0, docl = doc[:, 0:1], doc[:, T - 1 : T]
    mxf, mxb = mf[:, T - 1 : T], mb[:, 0:1]
    totf, totb = cumf[:, T - 1 : T], cumb[:, 0:1]
    wf = jnp.where(doc == docl, jnp.exp(af - mxf), 0.0)
    wbk = jnp.where(doc == doc0, jnp.exp(ab - mxb), 0.0)
    arow[0] = af
    arow[1] = ab
    arow[2] = doc
    stack = jnp.where(
        rowi == 0, mf,
        jnp.where(rowi == 1, mb, jnp.where(rowi == 2, doc, jnp.where(rowi == 3, wf, wbk))),
    )
    cols[...] = stack.T
    r8 = lax.broadcasted_iota(jnp.int32, (8, 128), 0)
    scal = jnp.zeros((8, 128), F32)
    for i, val in enumerate((totf + mxf, totb + mxb, totf, totb, doc0, docl)):
        scal = jnp.where(r8 == i, jnp.broadcast_to(val, (8, 128)), scal)
    sc_pair[c] = scal

    d_wd.wait_recv()
    ei = lax.broadcasted_iota(jnp.int32, (64, 128), 0)
    ej = lax.broadcasted_iota(jnp.int32, (64, 128), 1)
    put_own = jnp.where(ej == ei + 64 * c, 1.0, 0.0).astype(BF16)
    put_par = jnp.where(ej == ei + 64 * other, 1.0, 0.0).astype(BF16)
    mine = wa[pl.ds(pl.multiple_of(1024 * c, 1024), 1024), :]
    wd[z, y, c] = (
        jnp.dot(mine, put_own, preferred_element_type=F32)
        + jnp.dot(wb[...], put_par, preferred_element_type=F32)
    ).astype(BF16)
    b1.start()

    l_k.wait()
    l_v.wait()
    keys = k[...].astype(F32)
    for d in range(2):
        weighted = (keys * cols[:, 3 + d : 4 + d]).astype(BF16)
        st = lax.dot_general(
            v[...], weighted, (((0,), (0,)), ((), ())), preferred_element_type=F32
        ).astype(BF16)
        norm = jnp.sum(weighted.astype(F32), axis=0, keepdims=True)
        tail = jnp.broadcast_to(norm, (16, DK)).astype(BF16)
        for h in range(2):
            st_own[d, h, 0:256, :] = st[256 * h : 256 * h + 256]
            st_own[d, h, 256:SROWS, :] = tail
    d_st = cp.remote(st_own, st_par, partner)
    d_sc = cp.remote(sc_pair.at[c], sc_pair.at[c], partner)
    d_sc.start()
    d_st.start()
    a1.relay()

    def pick(ref, i):
        return ref[i : i + 1, 0:1]

    def pair_terms(s0, s1, d):
        early, late = (s0, s1) if d == 0 else (s1, s0)
        e_last = early[5 - d : 6 - d, 0:1]
        l_first, l_last = late[4 + d : 5 + d, 0:1], late[5 - d : 6 - d, 0:1]
        linked = (l_first == e_last) & (l_first == l_last)
        e_top = early[d : d + 1, 0:1] + late[2 + d : 3 + d, 0:1]
        l_top = late[d : d + 1, 0:1]
        top = jnp.where(linked, jnp.maximum(l_top, e_top), l_top)
        f_early = jnp.where(linked, jnp.exp(jnp.minimum(e_top - top, 0.0)), 0.0)
        f_late = jnp.exp(l_top - top)
        total = early[2 + d : 3 + d, 0:1] + late[2 + d : 3 + d, 0:1]
        return top, total, f_early, f_late, l_last

    d_sc.wait_recv()
    d_st.wait_recv()
    s0, s1 = sc_pair[0], sc_pair[1]
    cq = []
    cs = []
    for d in range(2):
        pos = c if d == 0 else other
        _, _, f_early, f_late, _ = pair_terms(s0, s1, d)
        f_own = jnp.where(pos == 0, f_early, f_late)
        f_par = jnp.where(pos == 0, f_late, f_early)
        q_send[d] = (f_own * st_own[d, c].astype(F32) + f_par * st_par[d, c].astype(F32)).astype(BF16)
        to = chip_up if d == 0 else chip_dn
        cs.append(cp.remote(sc_pair, sc_recv.at[d, 0], to))
        cq.append(cp.remote(q_send.at[d], q_recv.at[d, 0, c], to))
        cs[-1].start()
        cq[-1].start()

    l_q.wait()

    def intra(r0, size):
        qb = q[r0 : r0 + size, :]
        mfc, mbc, dc = (cols[r0 : r0 + size, i : i + 1] for i in range(3))
        score = (
            lax.dot_general(qb, k[...], (((1,), (1,)), ((), ())), preferred_element_type=F32)
            * SCALE
        )
        for d in range(2):
            lo, hi = (0, r0 + size) if d == 0 else (r0, T)
            ti = r0 + lax.broadcasted_iota(jnp.int32, (size, hi - lo), 0)
            si = lo + lax.broadcasted_iota(jnp.int32, (size, hi - lo), 1)
            keep = ((si <= ti) if d == 0 else (si >= ti)) & (arow[2, 0:1, lo:hi] == dc)
            e = jnp.exp(jnp.minimum(arow[d, 0:1, lo:hi] - (mfc if d == 0 else mbc), 0.0))
            w = jnp.where(keep, score[:, lo:hi] * e, 0.0)
            dens[r0 : r0 + size, d : d + 1] = jnp.sum(w, axis=1, keepdims=True)
            num = jnp.dot(w.astype(BF16), v[lo:hi, :], preferred_element_type=F32)
            (numf if d == 0 else numb)[r0 : r0 + size, :] = num

    intra(0, 256)
    a1.near()
    a1.far()
    a2.start()
    intra(256, 256)
    b1.relay()
    intra(512, 256)

    rq, rs, dq = [], [], []
    for d in range(2):
        to = chip_up if d == 0 else chip_dn
        rs.append(cp.remote(sc_recv.at[d, 0], sc_recv.at[d, 1], to))
        rq.append(cp.remote(q_recv.at[d, 0, c], q_recv.at[d, 1, c], to))
        dq.append(cp.remote(q_recv.at[d, 0, c], q_recv.at[d, 0, c], partner))
        cs[d].wait_recv()
        rs[d].start()
        cq[d].wait_recv()
        rq[d].start()
        dq[d].start()
    b1.near()
    b1.far()
    b2.start()
    wr.relay()

    fw = [
        cp.remote(wu.at[z, :, c], wu.at[z, :, c], partner),
        cp.remote(wd.at[:, y, c], wd.at[:, y, c], partner),
    ]
    for f in fw:
        f.start()

    dq2 = []
    for d in range(2):
        rs[d].wait_recv()
        rq[d].wait_recv()
        dq2.append(cp.remote(q_recv.at[d, 1, c], q_recv.at[d, 1, c], partner))
        dq2[d].start()

    scal_in = []
    for d in range(2):
        pos = c if d == 0 else other
        chip = n if d == 0 else 15 - n
        own_s = sc_pair[c]
        par_s = sc_pair[other]
        first = own_s[4 + d : 5 + d, 0:1]
        t1, tot1, _, _, last1 = pair_terms(sc_recv[d, 0, 0], sc_recv[d, 0, 1], d)
        t2, _, _, _, last2 = pair_terms(sc_recv[d, 1, 0], sc_recv[d, 1, 1], d)
        l0 = (par_s[5 - d : 6 - d, 0:1] == first) & (pos == 1)
        l1 = (last1 == first) & (chip >= 1)
        l2 = (last2 == first) & (chip >= 2)
        shift = jnp.where(pos == 1, par_s[2 + d : 3 + d, 0:1], 0.0)
        e0 = jnp.where(l0, par_s[d : d + 1, 0:1], FAR_LOW)
        e1 = jnp.where(l1, t1 + shift, FAR_LOW)
        e2 = jnp.where(l2, t2 + tot1 + shift, FAR_LOW)
        top = jnp.maximum(e0, jnp.maximum(e1, e2))
        g0 = jnp.where(l0, jnp.exp(e0 - top), 0.0)
        g1 = jnp.where(l1, jnp.exp(e1 - top), 0.0)
        g2 = jnp.where(l2, jnp.exp(e2 - top), 0.0)
        late = jnp.where(pos == 1, 1.0, 0.0)
        linked = late * jnp.where(l0, 1.0, 0.0) + (1.0 - late) * jnp.where(l1, 1.0, 0.0)
        dq[d].wait_recv()
        dq2[d].wait_recv()
        for h in range(2):
            cin[d, h] = (
                g0 * st_par[d, h].astype(F32)
                + g1 * q_recv[d, 0, h].astype(F32)
                + g2 * q_recv[d, 1, h].astype(F32)
            ).astype(BF16)
        scal_in.append((top, linked, first))

    l_og.wait()
    ca = []
    for step, to in enumerate((xf, xp, xm, x)):
        r0 = pl.multiple_of(to * ROWS, 64)
        rows = pl.ds(r0, ROWS)
        qb = q[rows, :]
        qw = qb.astype(F32)
        dc = cols[rows, 2:3]
        memory = None
        for d in range(2):
            top, linked, first = scal_in[d]
            m_loc = cols[rows, d : d + 1]
            usable = jnp.where(dc == first, linked, 0.0) > 0.5
            m = jnp.where(usable, jnp.maximum(m_loc, top), m_loc)
            keep = jnp.exp(m_loc - m)
            inter = jnp.where(usable, jnp.exp(jnp.minimum(top - m, 0.0)), 0.0) * SCALE
            nt = (((1,), (1,)), ((), ()))
            qc = jnp.concatenate(
                [
                    lax.dot_general(qb, cin[d, h, 0:256, :], nt, preferred_element_type=F32)
                    for h in range(2)
                ],
                axis=1,
            )
            norm = cin[d, 0, 256:257, :].astype(F32)
            num = keep * (numf if d == 0 else numb)[rows, :] + inter * qc
            den = keep * dens[rows, d : d + 1] + inter * jnp.sum(qw * norm, axis=1, keepdims=True)
            h_dir = num / jnp.maximum(jnp.abs(den), 1.0)
            memory = h_dir if memory is None else memory + h_dir
        normed = memory * lax.rsqrt(jnp.mean(memory * memory, axis=1, keepdims=True) + EPS)
        gate = 1.0 / (1.0 + jnp.exp(-og[rows, :].astype(F32)))
        readout = (normed * gain_ref[...] * gate).astype(BF16)
        if step < 3:
            ro_out[step] = readout
            cc = cp.remote(ro_out.at[step], ro.at[x], {"x": to})
            cc.start()
            ca.append(cc)
        else:
            ro[x] = readout

    a2.relay()
    wr.near()
    fo = [cp.remote(wo.at[p, c], wo.at[p, c], partner) for p in (xm, xp, xf)]
    fo[0].start()
    fo[1].start()
    b2.relay()
    wr.far()
    fo[2].start()
    l_re.wait()
    for cc in ca:
        cc.wait_recv()
    for f in fo:
        f.wait_recv()

    mixed[...] = resid[...].astype(F32)

    @pl.loop(0, 4)
    def _(t):
        cs_ = pl.ds(pl.multiple_of(t * 512, 512), 512)
        tot = mixed[:, cs_]
        for h in range(4):
            w = wo[h, :, :, cs_].reshape(512, 512)
            tot = tot + jnp.dot(ro[h], w, preferred_element_type=F32).astype(BF16).astype(F32)
        mixed[:, cs_] = tot

    mx = mixed[...]
    factor = lax.rsqrt(jnp.mean(mx * mx, axis=1, keepdims=True) + EPS)
    nrm[0] = (mx * factor * ngain_ref[...]).astype(BF16)

    h01 = lambda j, h: nrm.at[j, pl.ds(HALF * h, HALF)]
    ag = Ring(
        cp, {"x": xp}, {"x": xm},
        lambda h: h01(0, h),
        lambda h: h01(1 + h, 0),
        lambda h: h01(2 - h, 1),
        h01(1, 0), h01(1, 1), h01(3, 0), h01(3, 1),
    )
    ag.start()

    def forward(ring_wait, refs):
        ring_wait()
        out = [cp.remote(r, r, partner) for r in refs]
        for f in out:
            f.start()
        return out

    zp, zm, zf = lax.rem(z + 1, 4), lax.rem(z + 3, 4), lax.rem(z + 2, 4)
    yp, ym, yf = lax.rem(y + 1, 4), lax.rem(y + 3, 4), lax.rem(y + 2, 4)
    fw += forward(a2.near, [wu.at[zp, :, c], wu.at[zm, :, c]])
    fw += forward(b2.near, [wd.at[:, yp, c], wd.at[:, ym, c]])
    fw += forward(a2.far, [wu.at[zf, :, c]])
    fw += forward(b2.far, [wd.at[:, yf, c]])
    for f in fw:
        f.wait_recv()

    def mixer(j, sink):
        rows = nrm[j]

        @pl.loop(0, 4)
        def _(t):
            cs_ = pl.ds(pl.multiple_of(t * 512, 512), 512)
            w = wu[:, :, :, :, cs_].reshape(D, 512)
            pre = jnp.maximum(jnp.dot(rows, w, preferred_element_type=F32), 0.0)
            hid[:, cs_] = (pre * pre).astype(BF16)

        @pl.loop(0, 4)
        def _(t):
            cs_ = pl.ds(pl.multiple_of(t * 512, 512), 512)
            w = jnp.concatenate([wd[t, i].reshape(D, 128) for i in range(4)], axis=1)
            sink(cs_, jnp.dot(hid[...], w, preferred_element_type=F32))

    def add_own(cs_, val):
        mixed[:, cs_] += val

    def to_part(j):
        def sink(cs_, val):
            part[j, :, cs_] = val.astype(BF16)

        return sink

    def to_acc(cs_, val):
        acc2[:, cs_] = val

    mixer(0, add_own)
    ag.relay()
    mixer(1, to_part(0))
    lo, hi = pl.ds(0, HALF), pl.ds(HALF, HALF)
    rs1 = [
        cp.remote(part.at[0, hi], rs_in.at[0, hi], {"x": xp}),
        cp.remote(part.at[0, lo], rs_in.at[1, lo], {"x": xm}),
    ]
    for r in rs1:
        r.start()
    ag.near()
    mixer(2, to_acc)
    ag.far()
    mixer(3, to_part(1))
    rs2 = [
        cp.remote(part.at[1, lo], add_in.at[0], {"x": xp}),
        cp.remote(part.at[1, hi], add_in.at[1], {"x": xm}),
    ]
    for r in rs2:
        r.start()
    rs3 = [
        cp.remote(part.at[2, hi], rs_in.at[0, lo], {"x": xp}),
        cp.remote(part.at[2, lo], rs_in.at[1, hi], {"x": xm}),
    ]
    rs2[0].wait_recv()
    part[2, HALF:ROWS, :] = (acc2[HALF:ROWS, :] + add_in[0].astype(F32)).astype(BF16)
    rs3[0].start()
    rs2[1].wait_recv()
    part[2, 0:HALF, :] = (acc2[0:HALF, :] + add_in[1].astype(F32)).astype(BF16)
    rs3[1].start()
    for r in (*rs1, *rs3):
        r.wait_recv()
    out_ref[...] = (mixed[...] + rs_in[0].astype(F32) + rs_in[1].astype(F32)).astype(BF16)
    for r in cp.all:
        r.wait_send()


def shards(
    queries, keys, values, out_gate, input_gates, forget_gates, doc_ids,
    head_gain, w_out, resid, norm_gain, w_up, w_down,
):
    vmem = pl.BlockSpec(memory_space=pltpu.VMEM)
    hbm = pl.BlockSpec(memory_space=pl.ANY)
    return pl.pallas_call(
        kernel,
        out_shape=jax.ShapeDtypeStruct((ROWS, D), BF16),
        in_specs=[vmem] * 5 + [hbm] * 8,
        out_specs=vmem,
        scratch_shapes=[
            pltpu.VMEM((4, 4, 2, 64, D), BF16),
            pltpu.VMEM((4, 4, 2, 1024, 128), BF16),
            pltpu.VMEM((4, 2, 256, D), BF16),
            pltpu.VMEM((D, 64), BF16),
            pltpu.VMEM((1024, 64), BF16),
            pltpu.VMEM((T, DK), BF16),
            pltpu.VMEM((T, DK), BF16),
            pltpu.VMEM((T, DV), BF16),
            pltpu.VMEM((T, DV), BF16),
            pltpu.VMEM((ROWS, D), BF16),
            pltpu.VMEM((3, 8, T), F32),
            pltpu.VMEM((T, 8), F32),
            pltpu.VMEM((T, DV), F32),
            pltpu.VMEM((T, DV), F32),
            pltpu.VMEM((T, 8), F32),
            pltpu.VMEM((2, 2, SROWS, DK), BF16),
            pltpu.VMEM((2, 2, SROWS, DK), BF16),
            pltpu.VMEM((2, 8, 128), F32),
            pltpu.VMEM((2, SROWS, DK), BF16),
            pltpu.VMEM((2, 2, 2, SROWS, DK), BF16),
            pltpu.VMEM((2, 2, 2, 8, 128), F32),
            pltpu.VMEM((2, 2, SROWS, DK), BF16),
            pltpu.VMEM((3, ROWS, DV), BF16),
            pltpu.VMEM((4, ROWS, DV), BF16),
            pltpu.VMEM((ROWS, D), F32),
            pltpu.VMEM((4, ROWS, D), BF16),
            pltpu.VMEM((ROWS, D), BF16),
            pltpu.VMEM((3, ROWS, D), BF16),
            pltpu.VMEM((ROWS, D), F32),
            pltpu.VMEM((2, HALF, D), BF16),
            pltpu.VMEM((2, ROWS, D), BF16),
            pltpu.SemaphoreType.DMA((N_SEMS,)),
            pltpu.SemaphoreType.DMA((N_SEMS,)),
            pltpu.SemaphoreType.DMA((10,)),
        ],
        compiler_params=pltpu.CompilerParams(
            collective_id=0, has_side_effects=True, vmem_limit_bytes=66 * 1024 * 1000
        ),
        name="layer",
    )(
        input_gates, forget_gates, doc_ids.reshape(1, T), head_gain.reshape(1, DV),
        norm_gain.reshape(1, D), queries, keys, values, out_gate, w_out, resid, w_up, w_down,
    )


def solution(mesh):
    split = Mesh(mesh.devices.reshape(4, 4, 2, mesh.shape["tp"]), ("z", "y", "c", "x"))
    sp = ("z", "y", "c")
    return jax.shard_map(
        shards,
        mesh=split,
        in_specs=(
            P(sp, "x"), P(sp, "x"), P(sp, "x"), P(sp, "x"),
            P(None, "x", sp), P(None, "x", sp), P(sp), P("x"), P("x", None),
            P((*sp, "x"), None), P(), P(sp, "x"), P("x", sp),
        ),
        out_specs=P((*sp, "x"), None),
        check_vma=False,
    )
```

time: 502 us -> 139 us (0.28)
  waiting for transfers between devices: 138 us -> 0 us
  between operations: 134 us -> 0.01 us
  Pallas kernels: 0 us -> 131 us
  blocking collectives: 88.7 us -> 0 us
  local copies, waits for them, and re-layouts: 72.9 us -> 5.32 us
  matrix products: 43.3 us -> 0 us
  other arithmetic: 18.8 us -> 0 us
    all_gather x7 -> x0, waiting for transfers between devices: 137 us -> none  [the longest x1 55.2 us: fetch_weights(): up_full = lax.all_gather(w_up, SP, axis=0, tiled=True)]
    pallas_call x0 -> x1, Pallas kernels: none -> 131 us  [shards(): pl.pallas_call(kernel, out_shape=jax.ShapeDtypeStruct((ROWS, D), BF16), i...]
    all_to_all x2 -> x0, blocking collectives: 84.3 us -> none  [sent_and_summed(): lax.all_to_all(split_up(value, dim, length), axis, 0, 0, tiled=True)]
    dot_general x13 -> x0, matrix products: 43.3 us -> none  [the longest x1 11.9 us: shards(): jnp.dot(lax.all_gather(scaled, 'tp', axis=0, tiled=True), up_full, prefer...]
    another operation x7 -> x0, local copies, waits for them, and re-layouts: 35.8 us -> none
    slice x42 -> x0, local copies, waits for them, and re-layouts: 25 us -> none  [the longest x30 17.1 us: carried_in(): part[k].astype(own.dtype)]
    concatenate x6 -> x0, local copies, waits for them, and re-layouts: 5.77 us -> none  [gathered_once(): both, at, found = (lax.all_gather(jnp.concatenate(lines), axis), 0, {})]
  transfers between devices with their start and end apart: 7 -> 0, of which waited for: 3 -> 0; matrix products, arithmetic and copies ran while one was open for 14% -> 0% of each run, Pallas kernels for 0% -> 0%
where the time goes in v1:
time: 139 us; the launch traced here: 136 us
  Pallas kernels  131 us (94%)
  local copies, waits for them, and re-layouts  5.32 us (4%)
    pallas_call x1, Pallas kernels, shards(): pl.pallas_call(kernel, out_shape=jax.ShapeDtypeStruct((ROWS, D), BF16), i...  131 us
    unnamed x2, local copies, waits for them, and re-layouts  4.04 us

profile of v1, /device:TPU:0, one launch (start us, length us, event | category | flops | bytes accessed | tf_op | source)
XLA Modules:
  0.0 136.0 jit_solution(8278277869778519598)
XLA Ops:
  0.0 1.3 reshape.9.doc_ref
  1.3 2.0 %copy.14.wdn_h = bf16[2048,64]{1,0:T(8,128)(2,1)} copy(bf16[2048,64]{0,1:T(8,128)(2,1)} %param.25) | data formatting | bytes 524288 | tf_op args[12]
  3.2 130.6 %layer.1 = bf16[192,2048]{1,0:T(8,128)(2,1)} custom-call(f32[2,1,768]{2,1,0:T(1,128)} %ig_ref.1, f32[2,1,768]{2,1,0:T(1,128)} %fg_ref.1, s32[1,768]{1,0:T(1,128)} %reshape.9.doc_ref, f32[1,512]{1,0:T(1,128)} %bitcast.3, f32[1,2048]{1,0:T(1,128)} %bitcast.2, bf16[768,256]{1,0:T(8,128)(2,1)} %q_h.1, bf16[768,256]{1,0:T(8,128)(2,1)} %k_h.1, ...), custom_call_target="tpu_custom_call" | custom-call | tf_op jit(solution)/shard_map/layer/pallas_call | solution.py:516
  133.9 2.1 %copy.16 = bf16[192,2048]{1,0:T(8,128)(2,1)} copy(bf16[192,2048]{1,0:T(8,128)(2,1)} %layer.1) | data formatting | bytes 1572864

commit v2 on v1

--- a/solution.py
+++ b/solution.py
@@ -1,4 +1,4 @@
-import functools
+import contextlib
 
 import jax
 import jax.numpy as jnp
@@ -22,7 +22,17 @@
 D = 2048
 SROWS = 272
 SCALE = DK ** (-0.5)
-N_SEMS = 96
+N_SEMS = 112
+
+
+class Stages:
+    def __init__(self):
+        self.scopes = contextlib.ExitStack()
+
+    def __call__(self, name=None):
+        self.scopes.close()
+        if name:
+            self.scopes.enter_context(jax.named_scope(name))
 
 
 class Copies:
@@ -62,9 +72,17 @@
         self.rp = cp.remote(near0, far0, plus)
         self.rm = cp.remote(near1, far1, minus)
 
+    def start0(self):
+        self.p0.start()
+        self.m0.start()
+
+    def start1(self):
+        self.p1.start()
+        self.m1.start()
+
     def start(self):
-        for c in (self.p0, self.m0, self.p1, self.m1):
-            c.start()
+        self.start0()
+        self.start1()
 
     def relay(self):
         self.p0.wait_recv()
@@ -97,11 +115,11 @@
 def kernel(
     ig_ref, fg_ref, doc_ref, gain_ref, ngain_ref,
     q_h, k_h, v_h, og_h, wout_h, resid_h, wup_h, wdn_h,
-    out_ref,
-    wu, wd, wo, wa, wb, q, k, v, og, resid,
+    own_out, rs_in,
+    wu, wd, wox, wop, wa, wb, q, k, v, og, resid,
     arow, cols, numf, numb, dens,
     st_own, st_par, sc_pair, q_send, q_recv, sc_recv, cin,
-    ro_out, ro, mixed, nrm, hid, part, acc2, add_in, rs_in,
+    ro_out, ro_st, ro, mixed, nrm, hid, part, acc2, add_in,
     send_sem, recv_sem, loc_sem,
 ):
     z, y, c, x = (lax.axis_index(a) for a in ("z", "y", "c", "x"))
@@ -113,18 +131,24 @@
     partner = {"c": other}
     xp, xm, xf = lax.rem(x + 1, 4), lax.rem(x + 3, 4), lax.rem(x + 2, 4)
     cp = Copies(send_sem, recv_sem, loc_sem)
+    stage = Stages()
+    stage("loads")
 
     l_wd = cp.local(wdn_h, wa)
     l_wu = cp.local(wup_h, wu.at[z, y, c])
+    l_wo = [cp.local(wout_h.at[pl.ds(8 * i, 8)], wox.at[0, i]) for i in range(2)]
     l_k = cp.local(k_h, k)
     l_v = cp.local(v_h, v)
     l_q = cp.local(q_h, q)
-    l_wo = [cp.local(wout_h.at[pl.ds(256 * i, 256)], wo.at[x, i]) for i in range(2)]
     l_og = cp.local(og_h, og)
+    l_wp = [
+        cp.local(wout_h.at[pl.ds(16, 16), :, pl.ds(1024 * i, 1024)], wop.at[i, 0]) for i in range(2)
+    ]
     l_re = cp.local(resid_h, resid)
-    for l in (l_wd, l_wu, l_k, l_v, l_q, *l_wo, l_og, l_re):
+    for l in (l_wd, l_wu, *l_wo, l_k, l_v, l_q, l_og, *l_wp, l_re):
         l.start()
 
+    stage("barrier")
     barrier = pltpu.get_barrier_semaphore()
     peers = (
         partner, {"y": lax.rem(y + 1, 4)}, {"y": lax.rem(y + 3, 4)}, {"z": lax.rem(z + 1, 4)},
@@ -134,14 +158,59 @@
         pl.semaphore_signal(barrier, inc=1, device_id=dev, device_id_type=MESH)
     pl.semaphore_wait(barrier, len(peers))
 
+    stage("first_sends")
     a1 = slot_ring(cp, "y", y, lambda p, h: wu.at[z, p, c, pl.ds(32 * h, 32)])
     a2 = slot_ring(cp, "z", z, lambda p, h: wu.at[p, :, c, pl.ds(32 * h, 32)])
     b1 = slot_ring(cp, "z", z, lambda p, h: wd.at[p, y, c, pl.ds(512 * h, 512)])
     b2 = slot_ring(cp, "y", y, lambda p, h: wd.at[:, p, c, pl.ds(512 * h, 512)])
-    wr = slot_ring(cp, "x", x, lambda p, h: wo.at[p, c, pl.ds(128 * h, 128)])
-
+
+    wx = lambda j, h: wox.at[j, c, pl.ds(4 * h, 4)]
+    wr = Ring(
+        cp, {"x": xp}, {"x": xm},
+        lambda h: wx(0, h), lambda h: wx(3, h), lambda h: wx(1, h),
+        wx(3, 0), wx(1, 1), wx(2, 0), wx(2, 1),
+    )
+    a_pos, b_pos = jnp.where(c == 0, z, y), jnp.where(c == 0, y, z)
+    piece = a_pos * 4 + b_pos
+    cols_c = pl.ds(pl.multiple_of(1024 * c, 1024), 1024)
+    wp = [
+        cp.remote(wout_h.at[16 + piece, :, cols_c], wop.at[c, j, piece], {"x": to})
+        for to, j in ((xp, 3), (xm, 1), (xf, 2))
+    ]
+
+    def dev_b(step):
+        return {
+            "z": jnp.where(c == 0, z, lax.rem(z + step, 4)),
+            "y": jnp.where(c == 0, lax.rem(y + step, 4), y),
+        }
+
+    def dev_a(step):
+        return {
+            "z": jnp.where(c == 0, lax.rem(z + step, 4), z),
+            "y": jnp.where(c == 0, y, lax.rem(y + step, 4)),
+        }
+
+    def piece_ring(plus, minus, pos, slot):
+        own = lambda h: slot(pos, h)
+        up, down = lax.rem(pos + 1, 4), lax.rem(pos + 3, 4)
+        return Ring(
+            cp, plus, minus, own, own, own,
+            slot(down, 0), slot(up, 1), slot(down, 0), slot(up, 1),
+        )
+
+    c1 = piece_ring(
+        dev_b(1), dev_b(3), b_pos,
+        lambda p, h: wop.at[c, pl.ds(1, 3), a_pos * 4 + p, :, pl.ds(512 * h, 512)],
+    )
+    c2 = piece_ring(
+        dev_a(1), dev_a(3), a_pos,
+        lambda p, h: wop.at[c, pl.ds(1, 3), pl.ds(4 * p, 4), :, pl.ds(512 * h, 512)],
+    )
+
+    for w in wp:
+        w.start()
     l_wd.wait()
-    d_wd = cp.remote(wa.at[pl.ds(pl.multiple_of(1024 * other, 1024), 1024)], wb, partner)
+    d_wd = cp.remote(wa.at[:, pl.ds(pl.multiple_of(1024 * other, 1024), 1024)], wb, partner)
     d_wd.start()
     l_wu.wait()
     a1.start()
@@ -149,12 +218,13 @@
         l.wait()
     wr.start()
 
+    stage("gates")
     def row(ref, i):
         return jnp.broadcast_to(ref[i], (8, T))
 
     lane = lax.broadcasted_iota(jnp.int32, (8, T), 1)
     rowi = lax.broadcasted_iota(jnp.int32, (8, T), 0)
-    doc = jnp.broadcast_to(doc_ref[...], (8, T)).astype(F32)
+    doc = jnp.broadcast_to(doc_ref[...].astype(F32)[None, :], (8, T))
 
     def log_sigmoid(f):
         return jnp.minimum(f, 0.0) - jnp.log1p(jnp.exp(-jnp.abs(f)))
@@ -192,22 +262,28 @@
     for i, val in enumerate((totf + mxf, totb + mxb, totf, totb, doc0, docl)):
         scal = jnp.where(r8 == i, jnp.broadcast_to(val, (8, 128)), scal)
     sc_pair[c] = scal
-
+    d_sc = cp.remote(sc_pair.at[c], sc_pair.at[c], partner)
+    d_sc.start()
+
+    stage("wd_block")
     d_wd.wait_recv()
     ei = lax.broadcasted_iota(jnp.int32, (64, 128), 0)
     ej = lax.broadcasted_iota(jnp.int32, (64, 128), 1)
     put_own = jnp.where(ej == ei + 64 * c, 1.0, 0.0).astype(BF16)
     put_par = jnp.where(ej == ei + 64 * other, 1.0, 0.0).astype(BF16)
-    mine = wa[pl.ds(pl.multiple_of(1024 * c, 1024), 1024), :]
+    mine = wa[:, pl.ds(pl.multiple_of(1024 * c, 1024), 1024)]
+    tn = (((0,), (0,)), ((), ()))
     wd[z, y, c] = (
-        jnp.dot(mine, put_own, preferred_element_type=F32)
-        + jnp.dot(wb[...], put_par, preferred_element_type=F32)
+        lax.dot_general(mine, put_own, tn, preferred_element_type=F32)
+        + lax.dot_general(wb[...], put_par, tn, preferred_element_type=F32)
     ).astype(BF16)
     b1.start()
 
+    stage("state")
     l_k.wait()
     l_v.wait()
     keys = k[...].astype(F32)
+    d_st = []
     for d in range(2):
         weighted = (keys * cols[:, 3 + d : 4 + d]).astype(BF16)
         st = lax.dot_general(
@@ -218,12 +294,10 @@
         for h in range(2):
             st_own[d, h, 0:256, :] = st[256 * h : 256 * h + 256]
             st_own[d, h, 256:SROWS, :] = tail
-    d_st = cp.remote(st_own, st_par, partner)
-    d_sc = cp.remote(sc_pair.at[c], sc_pair.at[c], partner)
-    d_sc.start()
-    d_st.start()
-    a1.relay()
-
+        d_st.append(cp.remote(st_own.at[d], st_par.at[d], partner))
+        d_st[d].start()
+
+    stage("pair_wait")
     def pick(ref, i):
         return ref[i : i + 1, 0:1]
 
@@ -241,7 +315,6 @@
         return top, total, f_early, f_late, l_last
 
     d_sc.wait_recv()
-    d_st.wait_recv()
     s0, s1 = sc_pair[0], sc_pair[1]
     cq = []
     cs = []
@@ -250,6 +323,7 @@
         _, _, f_early, f_late, _ = pair_terms(s0, s1, d)
         f_own = jnp.where(pos == 0, f_early, f_late)
         f_par = jnp.where(pos == 0, f_late, f_early)
+        d_st[d].wait_recv()
         q_send[d] = (f_own * st_own[d, c].astype(F32) + f_par * st_par[d, c].astype(F32)).astype(BF16)
         to = chip_up if d == 0 else chip_dn
         cs.append(cp.remote(sc_pair, sc_recv.at[d, 0], to))
@@ -257,6 +331,7 @@
         cs[-1].start()
         cq[-1].start()
 
+    stage("intra0")
     l_q.wait()
 
     def intra(r0, size):
@@ -278,13 +353,21 @@
             (numf if d == 0 else numb)[r0 : r0 + size, :] = num
 
     intra(0, 256)
-    a1.near()
-    a1.far()
-    a2.start()
+    stage("pieces")
+    for w in wp:
+        w.wait_recv()
+    c1.start()
+    b1.relay()
+    stage("intra1")
     intra(256, 256)
-    b1.relay()
+    stage("wr_relay")
+    wr.relay()
+    stage("intra2")
     intra(512, 256)
 
+    stage("c1_relay")
+    c1.relay()
+    stage("carry_near")
     rq, rs, dq = [], [], []
     for d in range(2):
         to = chip_up if d == 0 else chip_dn
@@ -296,25 +379,38 @@
         cq[d].wait_recv()
         rq[d].start()
         dq[d].start()
+    a1.relay()
+    stage("c1_wait")
+    c1.near()
+    c1.far()
+    c2.start()
+    stage("b1_wait")
     b1.near()
     b1.far()
-    b2.start()
-    wr.relay()
-
-    fw = [
-        cp.remote(wu.at[z, :, c], wu.at[z, :, c], partner),
-        cp.remote(wd.at[:, y, c], wd.at[:, y, c], partner),
-    ]
-    for f in fw:
-        f.start()
-
+    stage("carry_far")
     dq2 = []
     for d in range(2):
         rs[d].wait_recv()
         rq[d].wait_recv()
         dq2.append(cp.remote(q_recv.at[d, 1, c], q_recv.at[d, 1, c], partner))
         dq2[d].start()
-
+    fw = [
+        cp.remote(wu.at[z, :, c], wu.at[z, :, c], partner),
+        cp.remote(wd.at[:, y, c], wd.at[:, y, c], partner),
+    ]
+
+    def second_phase():
+        stage("c2_relay")
+        c2.relay()
+        a1.near()
+        a1.far()
+        a2.start()
+        b2.start()
+        for f in fw:
+            f.start()
+        stage("emit_rest")
+
+    stage("carry_combine")
     scal_in = []
     for d in range(2):
         pos = c if d == 0 else other
@@ -347,8 +443,10 @@
             ).astype(BF16)
         scal_in.append((top, linked, first))
 
+    stage("emit")
     l_og.wait()
     ca = []
+    lo, hi = pl.ds(0, HALF), pl.ds(HALF, HALF)
     for step, to in enumerate((xf, xp, xm, x)):
         r0 = pl.multiple_of(to * ROWS, 64)
         rows = pl.ds(r0, ROWS)
@@ -379,37 +477,64 @@
         normed = memory * lax.rsqrt(jnp.mean(memory * memory, axis=1, keepdims=True) + EPS)
         gate = 1.0 / (1.0 + jnp.exp(-og[rows, :].astype(F32)))
         readout = (normed * gain_ref[...] * gate).astype(BF16)
-        if step < 3:
+        if step == 3:
+            ro[x] = readout
+        else:
             ro_out[step] = readout
-            cc = cp.remote(ro_out.at[step], ro.at[x], {"x": to})
-            cc.start()
-            ca.append(cc)
-        else:
-            ro[x] = readout
-
-    a2.relay()
+        if step == 0:
+            ca0 = [
+                cp.remote(ro_out.at[0, lo], ro_st.at[0], {"x": xp}),
+                cp.remote(ro_out.at[0, hi], ro_st.at[1], {"x": xm}),
+            ]
+            for cc in ca0:
+                cc.start()
+            second_phase()
+        elif step < 3:
+            ca.append(cp.remote(ro_out.at[step], ro.at[x], {"x": to}))
+            ca[-1].start()
+    stage("a2a_relay")
+    ca += [
+        cp.remote(ro_st.at[0], ro.at[xm, lo], {"x": xp}),
+        cp.remote(ro_st.at[1], ro.at[xp, hi], {"x": xm}),
+    ]
+    for i in range(2):
+        ca0[i].wait_recv()
+        ca[2 + i].start()
+
+    stage("wout_fwd")
     wr.near()
-    fo = [cp.remote(wo.at[p, c], wo.at[p, c], partner) for p in (xm, xp, xf)]
+    wr.far()
+    fo = [cp.remote(wox.at[pl.ds(1, 3), c], wox.at[pl.ds(1, 3), c], partner)]
     fo[0].start()
+    c2.near()
+    c2.far()
+    fo.append(cp.remote(wop.at[c, pl.ds(1, 3)], wop.at[c, pl.ds(1, 3)], partner))
     fo[1].start()
-    b2.relay()
-    wr.far()
-    fo[2].start()
+    stage("a2a_wait")
     l_re.wait()
+    for l in l_wp:
+        l.wait()
+    for f in fo:
+        f.wait_recv()
     for cc in ca:
         cc.wait_recv()
-    for f in fo:
-        f.wait_recv()
-
+
+    stage("wout")
     mixed[...] = resid[...].astype(F32)
 
     @pl.loop(0, 4)
     def _(t):
         cs_ = pl.ds(pl.multiple_of(t * 512, 512), 512)
         tot = mixed[:, cs_]
-        for h in range(4):
-            w = wo[h, :, :, cs_].reshape(512, 512)
-            tot = tot + jnp.dot(ro[h], w, preferred_element_type=F32).astype(BF16).astype(F32)
+        side = pl.ds(pl.multiple_of(lax.rem(t, 2) * 512, 512), 512)
+        for j in range(4):
+            head = ro.at[lax.rem(x + j, 4)]
+            w0 = wox[j, :, :, :, cs_].reshape(256, 512)
+            w1 = wop[lax.div(t, 2), j, :, :, side].reshape(256, 512)
+            one = jnp.dot(head[:, 0:256], w0, preferred_element_type=F32) + jnp.dot(
+                head[:, 256:512], w1, preferred_element_type=F32
+            )
+            tot = tot + one.astype(BF16).astype(F32)
         mixed[:, cs_] = tot
 
     mx = mixed[...]
@@ -425,24 +550,32 @@
         h01(1, 0), h01(1, 1), h01(3, 0), h01(3, 1),
     )
     ag.start()
-
-    def forward(ring_wait, refs):
-        ring_wait()
-        out = [cp.remote(r, r, partner) for r in refs]
-        for f in out:
-            f.start()
-        return out
+    stage("a2_relay")
+    a2.relay()
+    stage("b2_relay")
+    b2.relay()
+    stage("ag_relay")
+    ag.relay()
+
+    stage("a2b2_near")
+    def forward(refs):
+        for r in refs:
+            fw.append(cp.remote(r, r, partner))
+            fw[-1].start()
 
     zp, zm, zf = lax.rem(z + 1, 4), lax.rem(z + 3, 4), lax.rem(z + 2, 4)
     yp, ym, yf = lax.rem(y + 1, 4), lax.rem(y + 3, 4), lax.rem(y + 2, 4)
-    fw += forward(a2.near, [wu.at[zp, :, c], wu.at[zm, :, c]])
-    fw += forward(b2.near, [wd.at[:, yp, c], wd.at[:, ym, c]])
-    fw += forward(a2.far, [wu.at[zf, :, c]])
-    fw += forward(b2.far, [wd.at[:, yf, c]])
-    for f in fw:
-        f.wait_recv()
-
-    def mixer(j, sink):
+    a2.near()
+    forward([wu.at[zp, :, c], wu.at[zm, :, c]])
+    b2.near()
+    forward([wd.at[:, yp, c], wd.at[:, ym, c]])
+    stage("a2_far")
+    a2.far()
+    forward([wu.at[zf, :, c]])
+    for i in (0, 2, 3, 6):
+        fw[i].wait_recv()
+
+    def up(j):
         rows = nrm[j]
 
         @pl.loop(0, 4)
@@ -450,13 +583,14 @@
             cs_ = pl.ds(pl.multiple_of(t * 512, 512), 512)
             w = wu[:, :, :, :, cs_].reshape(D, 512)
             pre = jnp.maximum(jnp.dot(rows, w, preferred_element_type=F32), 0.0)
-            hid[:, cs_] = (pre * pre).astype(BF16)
-
-        @pl.loop(0, 4)
+            hid[j, :, cs_] = (pre * pre).astype(BF16)
+
+    def down(j, first, last, sink):
+        @pl.loop(first, last)
         def _(t):
             cs_ = pl.ds(pl.multiple_of(t * 512, 512), 512)
             w = jnp.concatenate([wd[t, i].reshape(D, 128) for i in range(4)], axis=1)
-            sink(cs_, jnp.dot(hid[...], w, preferred_element_type=F32))
+            sink(cs_, jnp.dot(hid[j], w, preferred_element_type=F32))
 
     def add_own(cs_, val):
         mixed[:, cs_] += val
@@ -470,41 +604,64 @@
     def to_acc(cs_, val):
         acc2[:, cs_] = val
 
-    mixer(0, add_own)
-    ag.relay()
-    mixer(1, to_part(0))
-    lo, hi = pl.ds(0, HALF), pl.ds(HALF, HALF)
+    stage("up1")
+    up(1)
+    stage("up0")
+    up(0)
+    stage("b2_far")
+    b2.far()
+    forward([wd.at[:, yf, c]])
+    for i in (1, 4, 5, 7):
+        fw[i].wait_recv()
+    stage("down1")
+    down(1, 0, 4, to_part(0))
     rs1 = [
         cp.remote(part.at[0, hi], rs_in.at[0, hi], {"x": xp}),
         cp.remote(part.at[0, lo], rs_in.at[1, lo], {"x": xm}),
     ]
     for r in rs1:
         r.start()
+    stage("down0")
+    down(0, 0, 4, add_own)
+    l_mx = cp.local(mixed, own_out)
+    l_mx.start()
+    stage("ag_far")
+    ag.far()
+    stage("up3")
+    up(3)
+    stage("down3")
+    rs2, rs3 = [], []
+    for i in range(2):
+        down(3, 2 * i, 2 * i + 2, to_part(1))
+        wide = pl.ds(1024 * i, 1024)
+        rs2.append(cp.remote(part.at[1, lo, wide], add_in.at[0, :, wide], {"x": xp}))
+        rs2.append(cp.remote(part.at[1, hi, wide], add_in.at[1, :, wide], {"x": xm}))
+        rs3.append(cp.remote(part.at[2, hi, wide], rs_in.at[0, lo, wide], {"x": xp}))
+        rs3.append(cp.remote(part.at[2, lo, wide], rs_in.at[1, hi, wide], {"x": xm}))
+        rs2[-2].start()
+        rs2[-1].start()
+    stage("ff2")
     ag.near()
-    mixer(2, to_acc)
-    ag.far()
-    mixer(3, to_part(1))
-    rs2 = [
-        cp.remote(part.at[1, lo], add_in.at[0], {"x": xp}),
-        cp.remote(part.at[1, hi], add_in.at[1], {"x": xm}),
-    ]
-    for r in rs2:
-        r.start()
-    rs3 = [
-        cp.remote(part.at[2, hi], rs_in.at[0, lo], {"x": xp}),
-        cp.remote(part.at[2, lo], rs_in.at[1, hi], {"x": xm}),
-    ]
-    rs2[0].wait_recv()
-    part[2, HALF:ROWS, :] = (acc2[HALF:ROWS, :] + add_in[0].astype(F32)).astype(BF16)
-    rs3[0].start()
-    rs2[1].wait_recv()
-    part[2, 0:HALF, :] = (acc2[0:HALF, :] + add_in[1].astype(F32)).astype(BF16)
-    rs3[1].start()
+    up(2)
+    down(2, 0, 4, to_acc)
+    for i in range(2):
+        stage(f"rs_add{i}")
+        lanes = slice(1024 * i, 1024 * i + 1024)
+        for side in range(2):
+            rs2[2 * i + side].wait_recv()
+            rows = slice(HALF, ROWS) if side == 0 else slice(0, HALF)
+            part[2, rows, lanes] = (
+                acc2[rows, lanes] + add_in[side, :, lanes].astype(F32)
+            ).astype(BF16)
+            rs3[2 * i + side].start()
+    stage("rs_wait")
     for r in (*rs1, *rs3):
         r.wait_recv()
-    out_ref[...] = (mixed[...] + rs_in[0].astype(F32) + rs_in[1].astype(F32)).astype(BF16)
+    l_mx.wait()
+    stage("drain")
     for r in cp.all:
         r.wait_send()
+    stage()
 
 
 def shards(
@@ -513,17 +670,21 @@
 ):
     vmem = pl.BlockSpec(memory_space=pltpu.VMEM)
     hbm = pl.BlockSpec(memory_space=pl.ANY)
-    return pl.pallas_call(
+    own, sums = pl.pallas_call(
         kernel,
-        out_shape=jax.ShapeDtypeStruct((ROWS, D), BF16),
+        out_shape=(
+            jax.ShapeDtypeStruct((ROWS, D), F32),
+            jax.ShapeDtypeStruct((2, ROWS, D), BF16),
+        ),
         in_specs=[vmem] * 5 + [hbm] * 8,
-        out_specs=vmem,
+        out_specs=(hbm, hbm),
         scratch_shapes=[
             pltpu.VMEM((4, 4, 2, 64, D), BF16),
             pltpu.VMEM((4, 4, 2, 1024, 128), BF16),
-            pltpu.VMEM((4, 2, 256, D), BF16),
-            pltpu.VMEM((D, 64), BF16),
-            pltpu.VMEM((1024, 64), BF16),
+            pltpu.VMEM((4, 2, 8, 16, D), BF16),
+            pltpu.VMEM((2, 4, 16, 16, 1024), BF16),
+            pltpu.VMEM((64, D), BF16),
+            pltpu.VMEM((64, 1024), BF16),
             pltpu.VMEM((T, DK), BF16),
             pltpu.VMEM((T, DK), BF16),
             pltpu.VMEM((T, DV), BF16),
@@ -542,26 +703,28 @@
             pltpu.VMEM((2, 2, 2, 8, 128), F32),
             pltpu.VMEM((2, 2, SROWS, DK), BF16),
             pltpu.VMEM((3, ROWS, DV), BF16),
+            pltpu.VMEM((2, HALF, DV), BF16),
             pltpu.VMEM((4, ROWS, DV), BF16),
             pltpu.VMEM((ROWS, D), F32),
             pltpu.VMEM((4, ROWS, D), BF16),
-            pltpu.VMEM((ROWS, D), BF16),
+            pltpu.VMEM((4, ROWS, D), BF16),
             pltpu.VMEM((3, ROWS, D), BF16),
             pltpu.VMEM((ROWS, D), F32),
             pltpu.VMEM((2, HALF, D), BF16),
-            pltpu.VMEM((2, ROWS, D), BF16),
             pltpu.SemaphoreType.DMA((N_SEMS,)),
             pltpu.SemaphoreType.DMA((N_SEMS,)),
-            pltpu.SemaphoreType.DMA((10,)),
+            pltpu.SemaphoreType.DMA((13,)),
         ],
         compiler_params=pltpu.CompilerParams(
             collective_id=0, has_side_effects=True, vmem_limit_bytes=66 * 1024 * 1000
         ),
         name="layer",
     )(
-        input_gates, forget_gates, doc_ids.reshape(1, T), head_gain.reshape(1, DV),
-        norm_gain.reshape(1, D), queries, keys, values, out_gate, w_out, resid, w_up, w_down,
-    )
+        input_gates, forget_gates, doc_ids, head_gain.reshape(1, DV),
+        norm_gain.reshape(1, D), queries, keys, values, out_gate, w_out.reshape(32, 16, D), resid, w_up,
+        w_down.T,
+    )
+    return (own + sums[0].astype(F32) + sums[1].astype(F32)).astype(BF16)
 
 
 def solution(mesh):

time: 139 us -> 115 us (0.83); the launches traced: 136 us -> 114 us
  Pallas kernels: 131 us -> 111 us
  local copies, waits for them, and re-layouts: 5.32 us -> 0 us
  other arithmetic: 0 us -> 3.05 us
    pallas_call x1, Pallas kernels: 131 us -> 111 us  [shards(): pl.pallas_call(kernel, out_shape=(jax.ShapeDtypeStruct((ROWS, D), F32), j...]
    unnamed x2 -> x0, local copies, waits for them, and re-layouts: 4.04 us -> none
    convert_element_type x0 -> x1, other arithmetic: none -> 3.05 us  [shards(): return (own + sums[0].astype(F32) + sums[1].astype(F32)).astype(BF16)]
where the time goes in v2:
time: 115 us; the launch traced here: 114 us
  Pallas kernels  111 us (97%)
  other arithmetic  3.05 us (3%)
    pallas_call x1, Pallas kernels, shards(): pl.pallas_call(kernel, out_shape=(jax.ShapeDtypeStruct((ROWS, D), F32), j...  111 us
    convert_element_type x1, other arithmetic, shards(): return (own + sums[0].astype(F32) + sums[1].astype(F32)).astype(BF16)  3.05 us

profile of v2, /device:TPU:0, one launch (start us, length us, event | category | flops | bytes accessed | tf_op | source)
XLA Modules:
  0.0 114.5 jit_solution(7638204182584026760)
XLA Ops:
  0.0 111.4 %layer.1 = (f32[192,2048]{1,0:T(8,128)}, bf16[2,192,2048]{2,1,0:T(8,128)(2,1)}) custom-call(f32[2,1,768]{2,1,0:T(1,128)} %ig_ref.1, f32[2,1,768]{2,1,0:T(1,128)} %fg_ref.1, s32[768]{0:T(1024)} %doc_ref.1, f32[1,512]{1,0:T(1,128)} %bitcast.13, f32[1,2048]{1,0:T(1,128)} %bitcast.12, bf16[768,256]{1,0:T(8,128)(2,1)} %q_h.1, bf16[768,256]{1,0:T(8,128)(2,1)} %k_h.1, ...), custom_call_target="tpu_custom_call" | custom-call | tf_op jit(solution)/shard_map/layer/pallas_call | solution.py:673
  111.4 3.0 %fusion = bf16[192,2048]{1,0:T(8,128)(2,1)} fusion(f32[192,2048]{1,0:T(8,128)} %get-tuple-element.7, bf16[2,192,2048]{2,1,0:T(8,128)(2,1)} %get-tuple-element.8), kind=kLoop, calls=%fused_computation.1 | loop fusion | flops 1966080 | bytes 3932160 | tf_op jit(solution)/shard_map/convert_element_type | solution.py:727

commit v3 on v2

--- a/solution.py
+++ b/solution.py
@@ -22,7 +22,7 @@
 D = 2048
 SROWS = 272
 SCALE = DK ** (-0.5)
-N_SEMS = 112
+N_SEMS = (37, 62, 14)
 
 
 class Stages:
@@ -38,73 +38,97 @@
 class Copies:
     def __init__(self, send, recv, loc):
         self.send, self.recv, self.loc = send, recv, loc
-        self.at = 0
-        self.at_loc = 0
-        self.all = []
-
-    def remote(self, src, dst, dev):
-        k = self.at
-        self.at += 1
-        assert k < N_SEMS
+        self.sends = self.recvs = self.locals = 0
+        self.drain = []
+
+    def new_send(self):
+        self.sends += 1
+        return self.send.at[self.sends - 1]
+
+    def new_recv(self):
+        self.recvs += 1
+        return self.recv.at[self.recvs - 1]
+
+    def remote(self, src, dst, dev, send=None, recv=None):
+        alone = send is None
         c = pltpu.make_async_remote_copy(
             src_ref=src,
             dst_ref=dst,
-            send_sem=self.send.at[k],
-            recv_sem=self.recv.at[k],
+            send_sem=self.new_send() if alone else send,
+            recv_sem=self.new_recv() if recv is None else recv,
             device_id=dev,
             device_id_type=MESH,
         )
-        self.all.append(c)
+        if alone:
+            self.drain.append(c)
         return c
 
+    def waiter(self, ref, send, recv):
+        return pltpu.make_async_remote_copy(
+            src_ref=ref,
+            dst_ref=ref,
+            send_sem=send,
+            recv_sem=recv,
+            device_id={"c": 1 - lax.axis_index("c")},
+            device_id_type=MESH,
+        )
+
+    def drain_later(self, ref, send, recv):
+        self.drain.append(self.waiter(ref, send, recv))
+
     def local(self, src, dst):
-        k = self.at_loc
-        self.at_loc += 1
-        return pltpu.make_async_copy(src, dst, self.loc.at[k])
+        self.locals += 1
+        return pltpu.make_async_copy(src, dst, self.loc.at[self.locals - 1])
 
 
 class Ring:
-    def __init__(self, cp, plus, minus, own, put_plus, put_minus, near0, near1, far0, far1):
-        self.p0 = cp.remote(own(0), put_plus(0), plus)
-        self.m0 = cp.remote(own(1), put_minus(1), minus)
-        self.p1 = cp.remote(own(1), put_plus(1), plus)
-        self.m1 = cp.remote(own(0), put_minus(0), minus)
-        self.rp = cp.remote(near0, far0, plus)
-        self.rm = cp.remote(near1, far1, minus)
+    def __init__(
+        self, cp, plus, minus, own, put_plus, put_minus, near0, near1, far0, far1, block, three
+    ):
+        send = cp.new_send()
+        self.first, self.second, self.third = (cp.new_recv() for _ in range(3))
+
+        def group(srcs, dsts, dev, recv):
+            return [cp.remote(s, d, dev, send, recv) for s, d in zip(srcs, dsts, strict=True)]
+
+        self.out0 = group(own(0), put_plus(0), plus, self.first)
+        self.out0 += group(own(1), put_minus(1), minus, self.first)
+        self.out1 = group(own(1), put_plus(1), plus, self.second)
+        self.out1 += group(own(0), put_minus(0), minus, self.second)
+        self.on = group(near0, far0, plus, self.third) + group(near1, far1, minus, self.third)
+        self.waits = [cp.waiter(block, send, r) for r in (self.first, self.second, self.third)]
+        cp.drain_later(three, send, self.first)
 
     def start0(self):
-        self.p0.start()
-        self.m0.start()
+        for c in self.out0:
+            c.start()
 
     def start1(self):
-        self.p1.start()
-        self.m1.start()
+        for c in self.out1:
+            c.start()
 
     def start(self):
         self.start0()
         self.start1()
 
     def relay(self):
-        self.p0.wait_recv()
-        self.rp.start()
-        self.m0.wait_recv()
-        self.rm.start()
+        self.waits[0].wait_recv()
+        for c in self.on:
+            c.start()
 
     def near(self):
-        self.p1.wait_recv()
-        self.m1.wait_recv()
+        self.waits[1].wait_recv()
 
     def far(self):
-        self.rp.wait_recv()
-        self.rm.wait_recv()
-
-
-def slot_ring(cp, axis, p, slot):
-    plus, minus = lax.rem(p + 1, 4), lax.rem(p + 3, 4)
-    own = lambda h: slot(p, h)
+        self.waits[2].wait_recv()
+
+
+def slot_ring(cp, plus, minus, p, slots, block, three):
+    up, down = lax.rem(p + 1, 4), lax.rem(p + 3, 4)
+    at = lambda pos, h: [f(pos, h) for f in slots]
+    own = lambda h: at(p, h)
     return Ring(
-        cp, {axis: plus}, {axis: minus}, own, own, own,
-        slot(minus, 0), slot(plus, 1), slot(minus, 0), slot(plus, 1),
+        cp, plus, minus, own, own, own, at(down, 0), at(up, 1), at(down, 0), at(up, 1), block, three
     )
 
 
@@ -136,13 +160,14 @@
 
     l_wd = cp.local(wdn_h, wa)
     l_wu = cp.local(wup_h, wu.at[z, y, c])
-    l_wo = [cp.local(wout_h.at[pl.ds(8 * i, 8)], wox.at[0, i]) for i in range(2)]
+    l_wo = [cp.local(wout_h.at[pl.ds(12 * i, 12)], wox.at[0, i]) for i in range(2)]
     l_k = cp.local(k_h, k)
     l_v = cp.local(v_h, v)
     l_q = cp.local(q_h, q)
     l_og = cp.local(og_h, og)
     l_wp = [
-        cp.local(wout_h.at[pl.ds(16, 16), :, pl.ds(1024 * i, 1024)], wop.at[i, 0]) for i in range(2)
+        cp.local(wout_h.at[pl.ds(24, 8), :, pl.ds(512 * i, 512)], wop.at[i // 2, 0, :, i % 2])
+        for i in range(4)
     ]
     l_re = cp.local(resid_h, resid)
     for l in (l_wd, l_wu, *l_wo, l_k, l_v, l_q, l_og, *l_wp, l_re):
@@ -159,24 +184,52 @@
     pl.semaphore_wait(barrier, len(peers))
 
     stage("first_sends")
-    a1 = slot_ring(cp, "y", y, lambda p, h: wu.at[z, p, c, pl.ds(32 * h, 32)])
-    a2 = slot_ring(cp, "z", z, lambda p, h: wu.at[p, :, c, pl.ds(32 * h, 32)])
-    b1 = slot_ring(cp, "z", z, lambda p, h: wd.at[p, y, c, pl.ds(512 * h, 512)])
-    b2 = slot_ring(cp, "y", y, lambda p, h: wd.at[:, p, c, pl.ds(512 * h, 512)])
-
-    wx = lambda j, h: wox.at[j, c, pl.ds(4 * h, 4)]
+    zp, zm, zf = lax.rem(z + 1, 4), lax.rem(z + 3, 4), lax.rem(z + 2, 4)
+    yp, ym, yf = lax.rem(y + 1, 4), lax.rem(y + 3, 4), lax.rem(y + 2, 4)
+    over_y, over_z = ({"y": yp}, {"y": ym}), ({"z": zp}, {"z": zm})
+    up_half = lambda a, b, h: wu.at[a, b, c, pl.ds(32 * h, 32)]
+    dn_half = lambda a, b, h: wd.at[a, b, c, pl.ds(512 * h, 512)]
+    three = pl.ds(0, 3)
+    a1 = slot_ring(
+        cp, *over_y, y, [lambda p, h: up_half(z, p, h)], wu.at[z, y, c], wu.at[z, three, c]
+    )
+    a2o = slot_ring(
+        cp, *over_z, z, [lambda p, h: up_half(p, y, h)], wu.at[z, y, c], wu.at[z, three, c]
+    )
+    a2 = slot_ring(
+        cp, *over_z, z, [lambda p, h, o=o: up_half(p, o, h) for o in (yp, ym, yf)],
+        wu.at[z, three, c], wu.at[three, three, c],
+    )
+    b1 = slot_ring(
+        cp, *over_z, z, [lambda p, h: dn_half(p, y, h)], wd.at[z, y, c], wd.at[z, three, c]
+    )
+    b2o = slot_ring(
+        cp, *over_y, y, [lambda p, h: dn_half(z, p, h)], wd.at[z, y, c], wd.at[z, three, c]
+    )
+    b2 = slot_ring(
+        cp, *over_y, y, [lambda p, h, o=o: dn_half(o, p, h) for o in (zp, zm, zf)],
+        wd.at[z, three, c], wd.at[three, three, c],
+    )
+
+    wx = lambda j, h: wox.at[j, c, pl.ds(6 * h, 6)]
     wr = Ring(
         cp, {"x": xp}, {"x": xm},
-        lambda h: wx(0, h), lambda h: wx(3, h), lambda h: wx(1, h),
-        wx(3, 0), wx(1, 1), wx(2, 0), wx(2, 1),
+        lambda h: [wx(0, h)], lambda h: [wx(3, h)], lambda h: [wx(1, h)],
+        [wx(3, 0)], [wx(1, 1)], [wx(2, 0)], [wx(2, 1)], wox.at[0, c], wox.at[three, c],
     )
     a_pos, b_pos = jnp.where(c == 0, z, y), jnp.where(c == 0, y, z)
-    piece = a_pos * 4 + b_pos
-    cols_c = pl.ds(pl.multiple_of(1024 * c, 1024), 1024)
+    piece = lambda a, b: (2 * a + lax.div(b, 2), lax.rem(b, 2))
+    p_row, p_col = piece(a_pos, b_pos)
+    cols_c = pl.ds(pl.multiple_of(1024 * c + 512 * p_col, 512), 512)
+    wp_send, wp_recv = cp.new_send(), cp.new_recv()
     wp = [
-        cp.remote(wout_h.at[16 + piece, :, cols_c], wop.at[c, j, piece], {"x": to})
+        cp.remote(
+            wout_h.at[24 + p_row, :, cols_c], wop.at[c, j, p_row, p_col], {"x": to}, wp_send, wp_recv
+        )
         for to, j in ((xp, 3), (xm, 1), (xf, 2))
     ]
+    wp_all = cp.waiter(wop.at[c, three, 0, 0], wp_send, wp_recv)
+    cp.drain.append(wp_all)
 
     def dev_b(step):
         return {
@@ -190,21 +243,16 @@
             "y": jnp.where(c == 0, y, lax.rem(y + step, 4)),
         }
 
-    def piece_ring(plus, minus, pos, slot):
-        own = lambda h: slot(pos, h)
-        up, down = lax.rem(pos + 1, 4), lax.rem(pos + 3, 4)
-        return Ring(
-            cp, plus, minus, own, own, own,
-            slot(down, 0), slot(up, 1), slot(down, 0), slot(up, 1),
-        )
-
-    c1 = piece_ring(
-        dev_b(1), dev_b(3), b_pos,
-        lambda p, h: wop.at[c, pl.ds(1, 3), a_pos * 4 + p, :, pl.ds(512 * h, 512)],
-    )
-    c2 = piece_ring(
-        dev_a(1), dev_a(3), a_pos,
-        lambda p, h: wop.at[c, pl.ds(1, 3), pl.ds(4 * p, 4), :, pl.ds(512 * h, 512)],
+    heads = pl.ds(1, 3)
+    c1 = slot_ring(
+        cp, dev_b(1), dev_b(3), b_pos,
+        [lambda p, h: wop.at[(c, heads, *piece(a_pos, p), slice(None), pl.ds(256 * h, 256))]],
+        wop.at[c, heads, 0, 0], wop.at[c, heads, three, 0],
+    )
+    c2 = slot_ring(
+        cp, dev_a(1), dev_a(3), a_pos,
+        [lambda p, h: wop.at[c, heads, pl.ds(2 * p, 2), :, :, pl.ds(256 * h, 256)]],
+        wop.at[c, heads, pl.ds(0, 2)], wop.at[c, heads, pl.ds(0, 6)],
     )
 
     for w in wp:
@@ -354,19 +402,17 @@
 
     intra(0, 256)
     stage("pieces")
-    for w in wp:
-        w.wait_recv()
+    wp_all.wait_recv()
     c1.start()
     b1.relay()
+    b2o.start0()
     stage("intra1")
     intra(256, 256)
-    stage("wr_relay")
-    wr.relay()
     stage("intra2")
     intra(512, 256)
-
     stage("c1_relay")
     c1.relay()
+    a2o.start0()
     stage("carry_near")
     rq, rs, dq = [], [], []
     for d in range(2):
@@ -379,12 +425,15 @@
         cq[d].wait_recv()
         rq[d].start()
         dq[d].start()
-    a1.relay()
+    b2o.start1()
+    a2o.start1()
+    stage("wr_relay")
+    wr.relay()
     stage("c1_wait")
     c1.near()
     c1.far()
     c2.start()
-    stage("b1_wait")
+    a1.relay()
     b1.near()
     b1.far()
     stage("carry_far")
@@ -394,20 +443,18 @@
         rq[d].wait_recv()
         dq2.append(cp.remote(q_recv.at[d, 1, c], q_recv.at[d, 1, c], partner))
         dq2[d].start()
+    fw_send, fw_up, fw_dn = cp.new_send(), cp.new_recv(), cp.new_recv()
     fw = [
-        cp.remote(wu.at[z, :, c], wu.at[z, :, c], partner),
-        cp.remote(wd.at[:, y, c], wd.at[:, y, c], partner),
+        cp.remote(wu.at[z, :, c], wu.at[z, :, c], partner, fw_send, fw_up),
+        cp.remote(wd.at[:, y, c], wd.at[:, y, c], partner, fw_send, fw_dn),
     ]
 
     def second_phase():
         stage("c2_relay")
         c2.relay()
-        a1.near()
-        a1.far()
-        a2.start()
+        a2o.relay()
+        b2o.relay()
         b2.start()
-        for f in fw:
-            f.start()
         stage("emit_rest")
 
     stage("carry_combine")
@@ -488,10 +535,15 @@
             ]
             for cc in ca0:
                 cc.start()
-            second_phase()
         elif step < 3:
             ca.append(cp.remote(ro_out.at[step], ro.at[x], {"x": to}))
             ca[-1].start()
+            if step == 1:
+                second_phase()
+    stage("a1_wait")
+    a1.near()
+    a1.far()
+    a2.start()
     stage("a2a_relay")
     ca += [
         cp.remote(ro_st.at[0], ro.at[xm, lo], {"x": xp}),
@@ -510,6 +562,8 @@
     c2.far()
     fo.append(cp.remote(wop.at[c, pl.ds(1, 3)], wop.at[c, pl.ds(1, 3)], partner))
     fo[1].start()
+    for f in fw:
+        f.start()
     stage("a2a_wait")
     l_re.wait()
     for l in l_wp:
@@ -526,13 +580,12 @@
     def _(t):
         cs_ = pl.ds(pl.multiple_of(t * 512, 512), 512)
         tot = mixed[:, cs_]
-        side = pl.ds(pl.multiple_of(lax.rem(t, 2) * 512, 512), 512)
         for j in range(4):
             head = ro.at[lax.rem(x + j, 4)]
-            w0 = wox[j, :, :, :, cs_].reshape(256, 512)
-            w1 = wop[lax.div(t, 2), j, :, :, side].reshape(256, 512)
-            one = jnp.dot(head[:, 0:256], w0, preferred_element_type=F32) + jnp.dot(
-                head[:, 256:512], w1, preferred_element_type=F32
+            w0 = wox[j, :, :, :, cs_].reshape(384, 512)
+            w1 = wop[lax.div(t, 2), j, :, lax.rem(t, 2)].reshape(128, 512)
+            one = jnp.dot(head[:, 0:384], w0, preferred_element_type=F32) + jnp.dot(
+                head[:, 384:512], w1, preferred_element_type=F32
             )
             tot = tot + one.astype(BF16).astype(F32)
         mixed[:, cs_] = tot
@@ -544,36 +597,38 @@
     h01 = lambda j, h: nrm.at[j, pl.ds(HALF * h, HALF)]
     ag = Ring(
         cp, {"x": xp}, {"x": xm},
-        lambda h: h01(0, h),
-        lambda h: h01(1 + h, 0),
-        lambda h: h01(2 - h, 1),
-        h01(1, 0), h01(1, 1), h01(3, 0), h01(3, 1),
+        lambda h: [h01(0, h)],
+        lambda h: [h01(1 + h, 0)],
+        lambda h: [h01(2 - h, 1)],
+        [h01(1, 0)], [h01(1, 1)], [h01(3, 0)], [h01(3, 1)], nrm.at[0], nrm.at[three],
     )
     ag.start()
     stage("a2_relay")
     a2.relay()
     stage("b2_relay")
     b2.relay()
+    stage("a2b2_near")
+    def forward(refs, recv):
+        for r in refs:
+            cp.remote(r, r, partner, fw_send, recv).start()
+
+    up_all = cp.waiter(wu.at[:, :, 0], fw_send, fw_up)
+    dn_all = cp.waiter(wd.at[:, :, 0], fw_send, fw_dn)
+    cp.drain_later(wu, fw_send, fw_up)
+    a2o.near()
+    a2.near()
+    forward([wu.at[zp, :, c], wu.at[zm, :, c]], fw_up)
+    stage("b2_near")
+    b2o.near()
+    b2.near()
+    forward([wd.at[:, yp, c], wd.at[:, ym, c]], fw_dn)
     stage("ag_relay")
     ag.relay()
-
-    stage("a2b2_near")
-    def forward(refs):
-        for r in refs:
-            fw.append(cp.remote(r, r, partner))
-            fw[-1].start()
-
-    zp, zm, zf = lax.rem(z + 1, 4), lax.rem(z + 3, 4), lax.rem(z + 2, 4)
-    yp, ym, yf = lax.rem(y + 1, 4), lax.rem(y + 3, 4), lax.rem(y + 2, 4)
-    a2.near()
-    forward([wu.at[zp, :, c], wu.at[zm, :, c]])
-    b2.near()
-    forward([wd.at[:, yp, c], wd.at[:, ym, c]])
     stage("a2_far")
+    a2o.far()
     a2.far()
-    forward([wu.at[zf, :, c]])
-    for i in (0, 2, 3, 6):
-        fw[i].wait_recv()
+    forward([wu.at[zf, :, c]], fw_up)
+    up_all.wait_recv()
 
     def up(j):
         rows = nrm[j]
@@ -609,15 +664,17 @@
     stage("up0")
     up(0)
     stage("b2_far")
+    b2o.far()
     b2.far()
-    forward([wd.at[:, yf, c]])
-    for i in (1, 4, 5, 7):
-        fw[i].wait_recv()
+    forward([wd.at[:, yf, c]], fw_dn)
+    dn_all.wait_recv()
     stage("down1")
     down(1, 0, 4, to_part(0))
+    rs_send, rs_recv = cp.new_send(), cp.new_recv()
+    cp.drain_later(nrm.at[three], rs_send, rs_recv)
     rs1 = [
-        cp.remote(part.at[0, hi], rs_in.at[0, hi], {"x": xp}),
-        cp.remote(part.at[0, lo], rs_in.at[1, lo], {"x": xm}),
+        cp.remote(part.at[0, hi], rs_in.at[0, hi], {"x": xp}, rs_send, rs_recv),
+        cp.remote(part.at[0, lo], rs_in.at[1, lo], {"x": xm}, rs_send, rs_recv),
     ]
     for r in rs1:
         r.start()
@@ -634,10 +691,16 @@
     for i in range(2):
         down(3, 2 * i, 2 * i + 2, to_part(1))
         wide = pl.ds(1024 * i, 1024)
-        rs2.append(cp.remote(part.at[1, lo, wide], add_in.at[0, :, wide], {"x": xp}))
-        rs2.append(cp.remote(part.at[1, hi, wide], add_in.at[1, :, wide], {"x": xm}))
-        rs3.append(cp.remote(part.at[2, hi, wide], rs_in.at[0, lo, wide], {"x": xp}))
-        rs3.append(cp.remote(part.at[2, lo, wide], rs_in.at[1, hi, wide], {"x": xm}))
+        rs2.append(cp.remote(part.at[1, lo, wide], add_in.at[0, :, wide], {"x": xp}, rs_send))
+        rs2.append(cp.remote(part.at[1, hi, wide], add_in.at[1, :, wide], {"x": xm}, rs_send))
+        for part_rows, side, to in ((hi, 0, xp), (lo, 1, xm)):
+            rs_rows = lo if side == 0 else hi
+            rs3.append(
+                cp.remote(
+                    part.at[2, part_rows, wide], rs_in.at[side, rs_rows, wide], {"x": to},
+                    rs_send, rs_recv,
+                )
+            )
         rs2[-2].start()
         rs2[-1].start()
     stage("ff2")
@@ -655,11 +718,11 @@
             ).astype(BF16)
             rs3[2 * i + side].start()
     stage("rs_wait")
-    for r in (*rs1, *rs3):
-        r.wait_recv()
+    cp.waiter(rs_in, rs_send, rs_recv).wait_recv()
     l_mx.wait()
     stage("drain")
-    for r in cp.all:
+    assert (cp.sends, cp.recvs, cp.locals) == N_SEMS, (cp.sends, cp.recvs, cp.locals)
+    for r in cp.drain:
         r.wait_send()
     stage()
 
@@ -681,8 +744,8 @@
         scratch_shapes=[
             pltpu.VMEM((4, 4, 2, 64, D), BF16),
             pltpu.VMEM((4, 4, 2, 1024, 128), BF16),
-            pltpu.VMEM((4, 2, 8, 16, D), BF16),
-            pltpu.VMEM((2, 4, 16, 16, 1024), BF16),
+            pltpu.VMEM((4, 2, 12, 16, D), BF16),
+            pltpu.VMEM((2, 4, 8, 2, 16, 512), BF16),
             pltpu.VMEM((64, D), BF16),
             pltpu.VMEM((64, 1024), BF16),
             pltpu.VMEM((T, DK), BF16),
@@ -711,9 +774,7 @@
             pltpu.VMEM((3, ROWS, D), BF16),
             pltpu.VMEM((ROWS, D), F32),
             pltpu.VMEM((2, HALF, D), BF16),
-            pltpu.SemaphoreType.DMA((N_SEMS,)),
-            pltpu.SemaphoreType.DMA((N_SEMS,)),
-            pltpu.SemaphoreType.DMA((13,)),
+            *(pltpu.SemaphoreType.DMA((k,)) for k in N_SEMS),
         ],
         compiler_params=pltpu.CompilerParams(
             collective_id=0, has_side_effects=True, vmem_limit_bytes=66 * 1024 * 1000

time: 115 us -> 108 us (0.939)
  Pallas kernels: 111 us -> 104 us
    pallas_call x1, Pallas kernels: 111 us -> 104 us  [shards(): pl.pallas_call(kernel, out_shape=(jax.ShapeDtypeStruct((ROWS, D), F32), j...]
where the time goes in v3:
time: 108 us; the launch traced here: 107 us
  Pallas kernels  104 us (96%)
  other arithmetic  3.05 us (3%)
    pallas_call x1, Pallas kernels, shards(): pl.pallas_call(kernel, out_shape=(jax.ShapeDtypeStruct((ROWS, D), F32), j...  104 us
    convert_element_type x1, other arithmetic, shards(): return (own + sums[0].astype(F32) + sums[1].astype(F32)).astype(BF16)  3.05 us

profile of v3, /device:TPU:0, one launch (start us, length us, event | category | flops | bytes accessed | tf_op | source)
XLA Modules:
  0.0 107.4 jit_solution(8325523989589670649)
XLA Ops:
  0.0 104.3 %layer.1 = (f32[192,2048]{1,0:T(8,128)}, bf16[2,192,2048]{2,1,0:T(8,128)(2,1)}) custom-call(f32[2,1,768]{2,1,0:T(1,128)} %ig_ref.1, f32[2,1,768]{2,1,0:T(1,128)} %fg_ref.1, s32[768]{0:T(1024)} %doc_ref.1, f32[1,512]{1,0:T(1,128)} %bitcast.13, f32[1,2048]{1,0:T(1,128)} %bitcast.12, bf16[768,256]{1,0:T(8,128)(2,1)} %q_h.1, bf16[768,256]{1,0:T(8,128)(2,1)} %k_h.1, ...), custom_call_target="tpu_custom_call" | custom-call | tf_op jit(solution)/shard_map/layer/pallas_call | solution.py:736
  104.3 3.0 %fusion = bf16[192,2048]{1,0:T(8,128)(2,1)} fusion(f32[192,2048]{1,0:T(8,128)} %get-tuple-element.7, bf16[2,192,2048]{2,1,0:T(8,128)(2,1)} %get-tuple-element.8), kind=kLoop, calls=%fused_computation.1 | loop fusion | flops 1966080 | bytes 3932160 | tf_op jit(solution)/shard_map/convert_element_type | solution.py:788

commit v4 on v3

--- a/solution.py
+++ b/solution.py
@@ -22,7 +22,9 @@
 D = 2048
 SROWS = 272
 SCALE = DK ** (-0.5)
-N_SEMS = (37, 62, 14)
+KP = 3
+WX = 16 - 2 * KP
+N_SEMS = (36, 63, 47)
 
 
 class Stages:
@@ -137,9 +139,10 @@
 
 
 def kernel(
-    ig_ref, fg_ref, doc_ref, gain_ref, ngain_ref,
+    ig_h, fg_h, doc_h, gain_h, ngain_h,
     q_h, k_h, v_h, og_h, wout_h, resid_h, wup_h, wdn_h,
     own_out, rs_in,
+    ig_ref, fg_ref, doc_ref, gain_ref, ngain_ref,
     wu, wd, wox, wop, wa, wb, q, k, v, og, resid,
     arow, cols, numf, numb, dens,
     st_own, st_par, sc_pair, q_send, q_recv, sc_recv, cin,
@@ -160,18 +163,24 @@
 
     l_wd = cp.local(wdn_h, wa)
     l_wu = cp.local(wup_h, wu.at[z, y, c])
-    l_wo = [cp.local(wout_h.at[pl.ds(12 * i, 12)], wox.at[0, i]) for i in range(2)]
+    l_wo = [cp.local(wout_h.at[pl.ds(WX * i, WX)], wox.at[0, i]) for i in range(2)]
     l_k = cp.local(k_h, k)
     l_v = cp.local(v_h, v)
     l_q = cp.local(q_h, q)
     l_og = cp.local(og_h, og)
     l_wp = [
-        cp.local(wout_h.at[pl.ds(24, 8), :, pl.ds(512 * i, 512)], wop.at[i // 2, 0, :, i % 2])
+        cp.local(
+            wout_h.at[pl.ds(2 * WX + KP * i, KP), :, pl.ds(1024 * j + 256 * b, 256)],
+            wop.at[j, 0, i, b],
+        )
         for i in range(4)
+        for j in range(2)
+        for b in range(4)
     ]
     l_re = cp.local(resid_h, resid)
-    for l in (l_wd, l_wu, *l_wo, l_k, l_v, l_q, l_og, *l_wp, l_re):
-        l.start()
+    l_gate = [cp.local(a, b) for a, b in ((ig_h, ig_ref), (fg_h, fg_ref), (doc_h, doc_ref))]
+    l_gain = [cp.local(gain_h, gain_ref), cp.local(ngain_h, ngain_ref)]
+    loads = (l_wu, *l_gate, l_wd, *l_wo, l_k, l_v, l_q, l_og, *l_gain, *l_wp, l_re)
 
     stage("barrier")
     barrier = pltpu.get_barrier_semaphore()
@@ -181,6 +190,8 @@
     )
     for dev in peers:
         pl.semaphore_signal(barrier, inc=1, device_id=dev, device_id_type=MESH)
+    for l in loads:
+        l.start()
     pl.semaphore_wait(barrier, len(peers))
 
     stage("first_sends")
@@ -211,20 +222,19 @@
         wd.at[z, three, c], wd.at[three, three, c],
     )
 
-    wx = lambda j, h: wox.at[j, c, pl.ds(6 * h, 6)]
+    wx = lambda j, h: wox.at[j, c, pl.ds(WX // 2 * h, WX // 2)]
     wr = Ring(
         cp, {"x": xp}, {"x": xm},
         lambda h: [wx(0, h)], lambda h: [wx(3, h)], lambda h: [wx(1, h)],
         [wx(3, 0)], [wx(1, 1)], [wx(2, 0)], [wx(2, 1)], wox.at[0, c], wox.at[three, c],
     )
     a_pos, b_pos = jnp.where(c == 0, z, y), jnp.where(c == 0, y, z)
-    piece = lambda a, b: (2 * a + lax.div(b, 2), lax.rem(b, 2))
-    p_row, p_col = piece(a_pos, b_pos)
-    cols_c = pl.ds(pl.multiple_of(1024 * c + 512 * p_col, 512), 512)
+    cols_c = pl.ds(pl.multiple_of(1024 * c + 256 * b_pos, 256), 256)
     wp_send, wp_recv = cp.new_send(), cp.new_recv()
     wp = [
         cp.remote(
-            wout_h.at[24 + p_row, :, cols_c], wop.at[c, j, p_row, p_col], {"x": to}, wp_send, wp_recv
+            wout_h.at[pl.ds(2 * WX + KP * a_pos, KP), :, cols_c], wop.at[c, j, a_pos, b_pos],
+            {"x": to}, wp_send, wp_recv,
         )
         for to, j in ((xp, 3), (xm, 1), (xf, 2))
     ]
@@ -246,27 +256,30 @@
     heads = pl.ds(1, 3)
     c1 = slot_ring(
         cp, dev_b(1), dev_b(3), b_pos,
-        [lambda p, h: wop.at[(c, heads, *piece(a_pos, p), slice(None), pl.ds(256 * h, 256))]],
-        wop.at[c, heads, 0, 0], wop.at[c, heads, three, 0],
+        [lambda p, h: wop.at[c, heads, a_pos, p, :, :, pl.ds(128 * h, 128)]],
+        wop.at[c, heads, 0, 0], wop.at[c, heads, 0, three],
     )
     c2 = slot_ring(
         cp, dev_a(1), dev_a(3), a_pos,
-        [lambda p, h: wop.at[c, heads, pl.ds(2 * p, 2), :, :, pl.ds(256 * h, 256)]],
-        wop.at[c, heads, pl.ds(0, 2)], wop.at[c, heads, pl.ds(0, 6)],
+        [lambda p, h: wop.at[c, heads, p, :, :, :, pl.ds(128 * h, 128)]],
+        wop.at[c, heads, 0], wop.at[c, heads, three],
     )
 
     for w in wp:
         w.start()
+    l_wu.wait()
+    a1.start0()
+    a2o.start0()
     l_wd.wait()
     d_wd = cp.remote(wa.at[:, pl.ds(pl.multiple_of(1024 * other, 1024), 1024)], wb, partner)
     d_wd.start()
-    l_wu.wait()
-    a1.start()
     for l in l_wo:
         l.wait()
     wr.start()
 
     stage("gates")
+    for l in l_gate:
+        l.wait()
     def row(ref, i):
         return jnp.broadcast_to(ref[i], (8, T))
 
@@ -313,20 +326,6 @@
     d_sc = cp.remote(sc_pair.at[c], sc_pair.at[c], partner)
     d_sc.start()
 
-    stage("wd_block")
-    d_wd.wait_recv()
-    ei = lax.broadcasted_iota(jnp.int32, (64, 128), 0)
-    ej = lax.broadcasted_iota(jnp.int32, (64, 128), 1)
-    put_own = jnp.where(ej == ei + 64 * c, 1.0, 0.0).astype(BF16)
-    put_par = jnp.where(ej == ei + 64 * other, 1.0, 0.0).astype(BF16)
-    mine = wa[:, pl.ds(pl.multiple_of(1024 * c, 1024), 1024)]
-    tn = (((0,), (0,)), ((), ()))
-    wd[z, y, c] = (
-        lax.dot_general(mine, put_own, tn, preferred_element_type=F32)
-        + lax.dot_general(wb[...], put_par, tn, preferred_element_type=F32)
-    ).astype(BF16)
-    b1.start()
-
     stage("state")
     l_k.wait()
     l_v.wait()
@@ -345,6 +344,20 @@
         d_st.append(cp.remote(st_own.at[d], st_par.at[d], partner))
         d_st[d].start()
 
+    stage("wd_block")
+    d_wd.wait_recv()
+    ei = lax.broadcasted_iota(jnp.int32, (64, 128), 0)
+    ej = lax.broadcasted_iota(jnp.int32, (64, 128), 1)
+    put_own = jnp.where(ej == ei + 64 * c, 1.0, 0.0).astype(BF16)
+    put_par = jnp.where(ej == ei + 64 * other, 1.0, 0.0).astype(BF16)
+    mine = wa[:, pl.ds(pl.multiple_of(1024 * c, 1024), 1024)]
+    tn = (((0,), (0,)), ((), ()))
+    wd[z, y, c] = (
+        lax.dot_general(mine, put_own, tn, preferred_element_type=F32)
+        + lax.dot_general(wb[...], put_par, tn, preferred_element_type=F32)
+    ).astype(BF16)
+    b1.start0()
+
     stage("pair_wait")
     def pick(ref, i):
         return ref[i : i + 1, 0:1]
@@ -404,15 +417,14 @@
     stage("pieces")
     wp_all.wait_recv()
     c1.start()
-    b1.relay()
-    b2o.start0()
+    b1.start1()
     stage("intra1")
     intra(256, 256)
     stage("intra2")
     intra(512, 256)
+
     stage("c1_relay")
     c1.relay()
-    a2o.start0()
     stage("carry_near")
     rq, rs, dq = [], [], []
     for d in range(2):
@@ -425,17 +437,18 @@
         cq[d].wait_recv()
         rq[d].start()
         dq[d].start()
-    b2o.start1()
-    a2o.start1()
+    stage("b1_relay")
+    b1.relay()
     stage("wr_relay")
     wr.relay()
     stage("c1_wait")
     c1.near()
     c1.far()
     c2.start()
+    a1.start1()
+    a2o.start1()
     a1.relay()
-    b1.near()
-    b1.far()
+
     stage("carry_far")
     dq2 = []
     for d in range(2):
@@ -443,18 +456,20 @@
         rq[d].wait_recv()
         dq2.append(cp.remote(q_recv.at[d, 1, c], q_recv.at[d, 1, c], partner))
         dq2[d].start()
-    fw_send, fw_up, fw_dn = cp.new_send(), cp.new_recv(), cp.new_recv()
-    fw = [
-        cp.remote(wu.at[z, :, c], wu.at[z, :, c], partner, fw_send, fw_up),
-        cp.remote(wd.at[:, y, c], wd.at[:, y, c], partner, fw_send, fw_dn),
-    ]
+    fw_send, fo_send = cp.new_send(), cp.new_send()
+    fw_up, fw_up2, fw_dn, fw_dn2, fo_recv = (cp.new_recv() for _ in range(5))
+
+    def forward(refs, recv, send=fw_send):
+        for r in refs:
+            cp.remote(r, r, partner, send, recv).start()
 
     def second_phase():
         stage("c2_relay")
         c2.relay()
+        b2o.start()
         a2o.relay()
-        b2o.relay()
-        b2.start()
+        wr.near()
+        forward([wox.at[j, c] for j in (1, 3)], fo_recv, fo_send)
         stage("emit_rest")
 
     stage("carry_combine")
@@ -491,7 +506,8 @@
         scal_in.append((top, linked, first))
 
     stage("emit")
-    l_og.wait()
+    for l in (l_og, *l_gain):
+        l.wait()
     ca = []
     lo, hi = pl.ds(0, HALF), pl.ds(HALF, HALF)
     for step, to in enumerate((xf, xp, xm, x)):
@@ -535,12 +551,14 @@
             ]
             for cc in ca0:
                 cc.start()
+            second_phase()
         elif step < 3:
             ca.append(cp.remote(ro_out.at[step], ro.at[x], {"x": to}))
             ca[-1].start()
-            if step == 1:
-                second_phase()
     stage("a1_wait")
+    b1.near()
+    b1.far()
+    b2.start()
     a1.near()
     a1.far()
     a2.start()
@@ -554,41 +572,47 @@
         ca[2 + i].start()
 
     stage("wout_fwd")
-    wr.near()
     wr.far()
-    fo = [cp.remote(wox.at[pl.ds(1, 3), c], wox.at[pl.ds(1, 3), c], partner)]
-    fo[0].start()
+    forward([wox.at[2, c]], fo_recv, fo_send)
     c2.near()
     c2.far()
-    fo.append(cp.remote(wop.at[c, pl.ds(1, 3)], wop.at[c, pl.ds(1, 3)], partner))
-    fo[1].start()
-    for f in fw:
-        f.start()
+    forward([wop.at[c, heads]], fo_recv, fo_send)
+    b2o.relay()
     stage("a2a_wait")
     l_re.wait()
     for l in l_wp:
         l.wait()
-    for f in fo:
-        f.wait_recv()
-    for cc in ca:
-        cc.wait_recv()
-
     stage("wout")
-    mixed[...] = resid[...].astype(F32)
-
-    @pl.loop(0, 4)
-    def _(t):
-        cs_ = pl.ds(pl.multiple_of(t * 512, 512), 512)
-        tot = mixed[:, cs_]
-        for j in range(4):
-            head = ro.at[lax.rem(x + j, 4)]
-            w0 = wox[j, :, :, :, cs_].reshape(384, 512)
-            w1 = wop[lax.div(t, 2), j, :, lax.rem(t, 2)].reshape(128, 512)
-            one = jnp.dot(head[:, 0:384], w0, preferred_element_type=F32) + jnp.dot(
-                head[:, 384:512], w1, preferred_element_type=F32
+
+    def project(j):
+        head = ro.at[lax.rem(x + j, 4)]
+        base = resid if j == 0 else mixed
+        for t in range(4):
+            cs_ = slice(512 * t, 512 * t + 512)
+            w0 = wox[j, :, :, :, cs_].reshape(512 - 64 * KP, 512)
+            at = [wop[t // 2, j, :, 2 * (t % 2) + i].reshape(64 * KP, 256) for i in range(2)]
+            one = jnp.dot(head[:, 0 : 512 - 64 * KP], w0, preferred_element_type=F32) + jnp.dot(
+                head[:, 512 - 64 * KP : 512],
+                jnp.concatenate(at, axis=1),
+                preferred_element_type=F32,
             )
-            tot = tot + one.astype(BF16).astype(F32)
-        mixed[:, cs_] = tot
+            mixed[:, cs_] = base[:, cs_].astype(F32) + one.astype(BF16).astype(F32)
+
+    project(0)
+    stage("fo_wait")
+    fo_all = cp.waiter(nrm, fo_send, fo_recv)
+    fo_all.wait_recv()
+    cp.drain.append(fo_all)
+    stage("near_wait")
+    ca[0].wait_recv()
+    project(3)
+    ca[1].wait_recv()
+    project(1)
+    stage("far_wait")
+    ca[2].wait_recv()
+    ca[3].wait_recv()
+    stage("far_project")
+    project(2)
 
     mx = mixed[...]
     factor = lax.rsqrt(jnp.mean(mx * mx, axis=1, keepdims=True) + EPS)
@@ -603,42 +627,34 @@
         [h01(1, 0)], [h01(1, 1)], [h01(3, 0)], [h01(3, 1)], nrm.at[0], nrm.at[three],
     )
     ag.start()
-    stage("a2_relay")
-    a2.relay()
-    stage("b2_relay")
-    b2.relay()
-    stage("a2b2_near")
-    def forward(refs, recv):
-        for r in refs:
-            cp.remote(r, r, partner, fw_send, recv).start()
-
-    up_all = cp.waiter(wu.at[:, :, 0], fw_send, fw_up)
-    dn_all = cp.waiter(wd.at[:, :, 0], fw_send, fw_dn)
+    up_most = cp.waiter(wu.at[three, :, 0], fw_send, fw_up)
+    up_last = cp.waiter(wu.at[0, :, 0], fw_send, fw_up2)
+    dn_most = cp.waiter(wd.at[three, :, 0], fw_send, fw_dn)
+    dn_last = cp.waiter(wd.at[0, :, 0], fw_send, fw_dn2)
     cp.drain_later(wu, fw_send, fw_up)
-    a2o.near()
-    a2.near()
-    forward([wu.at[zp, :, c], wu.at[zm, :, c]], fw_up)
-    stage("b2_near")
-    b2o.near()
-    b2.near()
-    forward([wd.at[:, yp, c], wd.at[:, ym, c]], fw_dn)
-    stage("ag_relay")
-    ag.relay()
-    stage("a2_far")
-    a2o.far()
-    a2.far()
-    forward([wu.at[zf, :, c]], fw_up)
-    up_all.wait_recv()
-
-    def up(j):
-        rows = nrm[j]
-
+
+    def up(j, zs, start=None, final=True):
         @pl.loop(0, 4)
         def _(t):
             cs_ = pl.ds(pl.multiple_of(t * 512, 512), 512)
-            w = wu[:, :, :, :, cs_].reshape(D, 512)
-            pre = jnp.maximum(jnp.dot(rows, w, preferred_element_type=F32), 0.0)
-            hid[j, :, cs_] = (pre * pre).astype(BF16)
+            if zs is None:
+                pre = jnp.dot(
+                    nrm[j], wu[:, :, :, :, cs_].reshape(D, 512), preferred_element_type=F32
+                )
+            else:
+                pre = start[:, cs_] if start is not None else None
+                for zz in zs:
+                    one = jnp.dot(
+                        nrm[j, :, pl.ds(pl.multiple_of(512 * zz, 512), 512)],
+                        wu[zz, :, :, :, cs_].reshape(512, 512),
+                        preferred_element_type=F32,
+                    )
+                    pre = one if pre is None else pre + one
+            if final:
+                pre = jnp.maximum(pre, 0.0)
+                hid[j, :, cs_] = (pre * pre).astype(BF16)
+            else:
+                acc2[:, cs_] = pre
 
     def down(j, first, last, sink):
         @pl.loop(first, last)
@@ -659,33 +675,80 @@
     def to_acc(cs_, val):
         acc2[:, cs_] = val
 
-    stage("up1")
-    up(1)
-    stage("up0")
-    up(0)
+    rs_send, rs_recv = cp.new_send(), cp.new_recv()
+    cp.drain_later(nrm.at[three], rs_send, rs_recv)
+
+    def first_sums(yy):
+        w = jnp.concatenate([wd[i, yy].reshape(D, 128) for i in range(4)], axis=1)
+        val = jnp.dot(hid[1], w, preferred_element_type=F32).astype(BF16)
+        for i in range(4):
+            strip = pl.ds(pl.multiple_of((4 * i + yy) * 128, 128), 128)
+            part[0, :, strip] = val[:, 128 * i : 128 * i + 128]
+        for i in range(4):
+            strip = pl.ds(pl.multiple_of((4 * i + yy) * 128, 128), 128)
+            for rows, side, to in ((hi, 0, xp), (lo, 1, xm)):
+                cp.remote(
+                    part.at[0, rows, strip], rs_in.at[side, rows, strip], {"x": to}, rs_send, rs_recv
+                ).start()
+
+    up_other, dn_other = (yp, ym, yf), (zp, zm, zf)
+    lower, upper = [pl.ds(32 * h, 32) for h in range(2)], [pl.ds(512 * h, 512) for h in range(2)]
+
+    def up_part(row, h):
+        return [wu.at[row, o, c, lower[h]] for o in up_other]
+
+    def dn_part(col, h):
+        return [wd.at[o, col, c, upper[h]] for o in dn_other]
+
+    stage("own_rows")
+    forward([wu.at[z, :, c]], fw_up)
+    forward([wd.at[:, y, c]], fw_dn)
+    a2o.near()
+    a2o.far()
+    forward([wu.at[zp, y, c], wu.at[zm, y, c]], fw_up)
+    forward([wu.at[zf, y, c]], fw_up2)
+    stage("a2_relay")
+    a2.relay()
+    forward(up_part(zm, 0) + up_part(zp, 1), fw_up)
+    stage("b2_relay")
+    b2o.near()
+    b2.relay()
+    forward([wd.at[z, yp, c], wd.at[z, ym, c]], fw_dn)
+    forward(dn_part(ym, 0) + dn_part(yp, 1), fw_dn)
+    stage("a2_near")
+    a2.near()
+    forward(up_part(zm, 1) + up_part(zp, 0), fw_up)
+    stage("b2_near")
+    b2.near()
+    forward(dn_part(ym, 1) + dn_part(yp, 0), fw_dn)
+    stage("ag_relay")
+    ag.relay()
+    stage("up1_most")
+    up_most.wait_recv()
+    up(1, (z, zp, zm), final=False)
+    stage("a2_far")
+    a2.far()
+    forward(up_part(zf, 0) + up_part(zf, 1), fw_up2)
+    up_last.wait_recv()
+    stage("up1_last")
+    up(1, (zf,), start=acc2)
+    stage("down1_most")
+    dn_most.wait_recv()
+    for yy in (y, yp, ym):
+        first_sums(yy)
     stage("b2_far")
     b2o.far()
     b2.far()
-    forward([wd.at[:, yf, c]], fw_dn)
-    dn_all.wait_recv()
-    stage("down1")
-    down(1, 0, 4, to_part(0))
-    rs_send, rs_recv = cp.new_send(), cp.new_recv()
-    cp.drain_later(nrm.at[three], rs_send, rs_recv)
-    rs1 = [
-        cp.remote(part.at[0, hi], rs_in.at[0, hi], {"x": xp}, rs_send, rs_recv),
-        cp.remote(part.at[0, lo], rs_in.at[1, lo], {"x": xm}, rs_send, rs_recv),
-    ]
-    for r in rs1:
-        r.start()
-    stage("down0")
-    down(0, 0, 4, add_own)
-    l_mx = cp.local(mixed, own_out)
-    l_mx.start()
+    forward([wd.at[:, yf, c]], fw_dn2)
+    stage("up0")
+    up(0, None)
+    stage("down1_last")
+    dn_last.wait_recv()
+    first_sums(yf)
     stage("ag_far")
     ag.far()
     stage("up3")
-    up(3)
+    up(3, None)
     stage("down3")
     rs2, rs3 = [], []
     for i in range(2):
@@ -705,7 +768,7 @@
         rs2[-1].start()
     stage("ff2")
     ag.near()
-    up(2)
+    up(2, None)
     down(2, 0, 4, to_acc)
     for i in range(2):
         stage(f"rs_add{i}")
@@ -717,6 +780,10 @@
                 acc2[rows, lanes] + add_in[side, :, lanes].astype(F32)
             ).astype(BF16)
             rs3[2 * i + side].start()
+    stage("down0")
+    down(0, 0, 4, add_own)
+    l_mx = cp.local(mixed, own_out)
+    l_mx.start()
     stage("rs_wait")
     cp.waiter(rs_in, rs_send, rs_recv).wait_recv()
     l_mx.wait()
@@ -731,7 +798,6 @@
     queries, keys, values, out_gate, input_gates, forget_gates, doc_ids,
     head_gain, w_out, resid, norm_gain, w_up, w_down,
 ):
-    vmem = pl.BlockSpec(memory_space=pltpu.VMEM)
     hbm = pl.BlockSpec(memory_space=pl.ANY)
     own, sums = pl.pallas_call(
         kernel,
@@ -739,13 +805,18 @@
             jax.ShapeDtypeStruct((ROWS, D), F32),
             jax.ShapeDtypeStruct((2, ROWS, D), BF16),
         ),
-        in_specs=[vmem] * 5 + [hbm] * 8,
+        in_specs=[hbm] * 13,
         out_specs=(hbm, hbm),
         scratch_shapes=[
+            pltpu.VMEM((2, 1, T), F32),
+            pltpu.VMEM((2, 1, T), F32),
+            pltpu.VMEM((T,), jnp.int32),
+            pltpu.VMEM((1, DV), F32),
+            pltpu.VMEM((1, D), F32),
             pltpu.VMEM((4, 4, 2, 64, D), BF16),
             pltpu.VMEM((4, 4, 2, 1024, 128), BF16),
-            pltpu.VMEM((4, 2, 12, 16, D), BF16),
-            pltpu.VMEM((2, 4, 8, 2, 16, 512), BF16),
+            pltpu.VMEM((4, 2, WX, 16, D), BF16),
+            pltpu.VMEM((2, 4, 4, 4, KP, 16, 256), BF16),
             pltpu.VMEM((64, D), BF16),
             pltpu.VMEM((64, 1024), BF16),
             pltpu.VMEM((T, DK), BF16),

time: 108 us -> 101 us (0.935)
  Pallas kernels: 104 us -> 96.6 us
    pallas_call x1, Pallas kernels: 104 us -> 96.6 us  [shards(): pl.pallas_call(kernel, out_shape=(jax.ShapeDtypeStruct((ROWS, D), F32), j...]
where the time goes in v4:
time: 101 us; the launch traced here: 99.6 us
  Pallas kernels  96.6 us (96%)
  other arithmetic  3.05 us (3%)
    pallas_call x1, Pallas kernels, shards(): pl.pallas_call(kernel, out_shape=(jax.ShapeDtypeStruct((ROWS, D), F32), j...  96.6 us
    convert_element_type x1, other arithmetic, shards(): return (own + sums[0].astype(F32) + sums[1].astype(F32)).astype(BF16)  3.05 us

profile of v4, /device:TPU:0, one launch (start us, length us, event | category | flops | bytes accessed | tf_op | source)
XLA Modules:
  0.0 99.6 jit_solution(206200857361883338)
XLA Ops:
  0.0 96.6 %layer.1 = (f32[192,2048]{1,0:T(8,128)}, bf16[2,192,2048]{2,1,0:T(8,128)(2,1)}) custom-call(f32[2,1,768]{2,1,0:T(1,128)} %ig_h.1, f32[2,1,768]{2,1,0:T(1,128)} %fg_h.1, s32[768]{0:T(1024)} %doc_h.1, f32[1,512]{1,0:T(1,128)} %bitcast.13, f32[1,2048]{1,0:T(1,128)} %bitcast.12, bf16[768,256]{1,0:T(8,128)(2,1)} %q_h.1, bf16[768,256]{1,0:T(8,128)(2,1)} %k_h.1, ...), custom_call_target="tpu_custom_call" | custom-call | tf_op jit(solution)/shard_map/layer/pallas_call | solution.py:802
  96.6 3.0 %fusion = bf16[192,2048]{1,0:T(8,128)(2,1)} fusion(f32[192,2048]{1,0:T(8,128)} %get-tuple-element.7, bf16[2,192,2048]{2,1,0:T(8,128)(2,1)} %get-tuple-element.8), kind=kLoop, calls=%fused_computation.1 | loop fusion | flops 1966080 | bytes 3932160 | tf_op jit(solution)/shard_map/convert_element_type | solution.py:859

commit v5 on v4

--- a/solution.py
+++ b/solution.py
@@ -24,7 +24,7 @@
 SCALE = DK ** (-0.5)
 KP = 3
 WX = 16 - 2 * KP
-N_SEMS = (36, 63, 47)
+N_SEMS = (20, 60, 16)
 
 
 class Stages:
@@ -78,8 +78,8 @@
     def drain_later(self, ref, send, recv):
         self.drain.append(self.waiter(ref, send, recv))
 
-    def local(self, src, dst):
-        self.locals += 1
+    def local(self, src, dst, again=False):
+        self.locals += not again
         return pltpu.make_async_copy(src, dst, self.loc.at[self.locals - 1])
 
 
@@ -172,11 +172,13 @@
         cp.local(
             wout_h.at[pl.ds(2 * WX + KP * i, KP), :, pl.ds(1024 * j + 256 * b, 256)],
             wop.at[j, 0, i, b],
+            i + j + b > 0,
         )
         for i in range(4)
         for j in range(2)
         for b in range(4)
     ]
+    l_wp_all = cp.local(wop.at[:, 0], wop.at[:, 0], True)
     l_re = cp.local(resid_h, resid)
     l_gate = [cp.local(a, b) for a, b in ((ig_h, ig_ref), (fg_h, fg_ref), (doc_h, doc_ref))]
     l_gain = [cp.local(gain_h, gain_ref), cp.local(ngain_h, ngain_ref)]
@@ -331,6 +333,7 @@
     l_v.wait()
     keys = k[...].astype(F32)
     d_st = []
+    st_send, q_sends, sc_sends, ro_send = (cp.new_send() for _ in range(4))
     for d in range(2):
         weighted = (keys * cols[:, 3 + d : 4 + d]).astype(BF16)
         st = lax.dot_general(
@@ -341,7 +344,7 @@
         for h in range(2):
             st_own[d, h, 0:256, :] = st[256 * h : 256 * h + 256]
             st_own[d, h, 256:SROWS, :] = tail
-        d_st.append(cp.remote(st_own.at[d], st_par.at[d], partner))
+        d_st.append(cp.remote(st_own.at[d], st_par.at[d], partner, st_send))
         d_st[d].start()
 
     stage("wd_block")
@@ -387,8 +390,8 @@
         d_st[d].wait_recv()
         q_send[d] = (f_own * st_own[d, c].astype(F32) + f_par * st_par[d, c].astype(F32)).astype(BF16)
         to = chip_up if d == 0 else chip_dn
-        cs.append(cp.remote(sc_pair, sc_recv.at[d, 0], to))
-        cq.append(cp.remote(q_send.at[d], q_recv.at[d, 0, c], to))
+        cs.append(cp.remote(sc_pair, sc_recv.at[d, 0], to, sc_sends))
+        cq.append(cp.remote(q_send.at[d], q_recv.at[d, 0, c], to, q_sends))
         cs[-1].start()
         cq[-1].start()
 
@@ -426,12 +429,12 @@
     stage("c1_relay")
     c1.relay()
     stage("carry_near")
-    rq, rs, dq = [], [], []
+    rq, rs, dq, dq_recv = [], [], [], cp.new_recv()
     for d in range(2):
         to = chip_up if d == 0 else chip_dn
-        rs.append(cp.remote(sc_recv.at[d, 0], sc_recv.at[d, 1], to))
-        rq.append(cp.remote(q_recv.at[d, 0, c], q_recv.at[d, 1, c], to))
-        dq.append(cp.remote(q_recv.at[d, 0, c], q_recv.at[d, 0, c], partner))
+        rs.append(cp.remote(sc_recv.at[d, 0], sc_recv.at[d, 1], to, sc_sends))
+        rq.append(cp.remote(q_recv.at[d, 0, c], q_recv.at[d, 1, c], to, q_sends))
+        dq.append(cp.remote(q_recv.at[d, 0, c], q_recv.at[d, 0, c], partner, q_sends, dq_recv))
         cs[d].wait_recv()
         rs[d].start()
         cq[d].wait_recv()
@@ -446,18 +449,21 @@
     c1.far()
     c2.start()
     a1.start1()
-    a2o.start1()
     a1.relay()
+    fo_send, fo_recv = cp.new_send(), cp.new_recv()
+    cp.remote(
+        wop.at[c, heads, a_pos], wop.at[c, heads, a_pos], partner, fo_send, fo_recv
+    ).start()
 
     stage("carry_far")
     dq2 = []
     for d in range(2):
         rs[d].wait_recv()
         rq[d].wait_recv()
-        dq2.append(cp.remote(q_recv.at[d, 1, c], q_recv.at[d, 1, c], partner))
+        dq2.append(cp.remote(q_recv.at[d, 1, c], q_recv.at[d, 1, c], partner, q_sends, dq_recv))
         dq2[d].start()
-    fw_send, fo_send = cp.new_send(), cp.new_send()
-    fw_up, fw_up2, fw_dn, fw_dn2, fo_recv = (cp.new_recv() for _ in range(5))
+    fw_send = cp.new_send()
+    fw_up, fw_up2, fw_dn, fw_dn2 = (cp.new_recv() for _ in range(4))
 
     def forward(refs, recv, send=fw_send):
         for r in refs:
@@ -466,6 +472,7 @@
     def second_phase():
         stage("c2_relay")
         c2.relay()
+        a2o.start1()
         b2o.start()
         a2o.relay()
         wr.near()
@@ -495,8 +502,8 @@
         g2 = jnp.where(l2, jnp.exp(e2 - top), 0.0)
         late = jnp.where(pos == 1, 1.0, 0.0)
         linked = late * jnp.where(l0, 1.0, 0.0) + (1.0 - late) * jnp.where(l1, 1.0, 0.0)
-        dq[d].wait_recv()
-        dq2[d].wait_recv()
+        if d == 0:
+            cp.waiter(q_recv.at[:, :, 0], q_sends, dq_recv).wait_recv()
         for h in range(2):
             cin[d, h] = (
                 g0 * st_par[d, h].astype(F32)
@@ -546,15 +553,16 @@
             ro_out[step] = readout
         if step == 0:
             ca0 = [
-                cp.remote(ro_out.at[0, lo], ro_st.at[0], {"x": xp}),
-                cp.remote(ro_out.at[0, hi], ro_st.at[1], {"x": xm}),
+                cp.remote(ro_out.at[0, lo], ro_st.at[0], {"x": xp}, ro_send),
+                cp.remote(ro_out.at[0, hi], ro_st.at[1], {"x": xm}, ro_send),
             ]
             for cc in ca0:
                 cc.start()
-            second_phase()
         elif step < 3:
-            ca.append(cp.remote(ro_out.at[step], ro.at[x], {"x": to}))
+            ca.append(cp.remote(ro_out.at[step], ro.at[x], {"x": to}, ro_send))
             ca[-1].start()
+            if step == 1:
+                second_phase()
     stage("a1_wait")
     b1.near()
     b1.far()
@@ -564,24 +572,25 @@
     a2.start()
     stage("a2a_relay")
     ca += [
-        cp.remote(ro_st.at[0], ro.at[xm, lo], {"x": xp}),
-        cp.remote(ro_st.at[1], ro.at[xp, hi], {"x": xm}),
+        cp.remote(ro_st.at[0], ro.at[xm, lo], {"x": xp}, ro_send),
+        cp.remote(ro_st.at[1], ro.at[xp, hi], {"x": xm}, ro_send),
     ]
     for i in range(2):
         ca0[i].wait_recv()
         ca[2 + i].start()
 
     stage("wout_fwd")
+    c2.near()
+    forward([wop.at[c, heads, lax.rem(a_pos + i, 4)] for i in (1, 3)], fo_recv, fo_send)
     wr.far()
     forward([wox.at[2, c]], fo_recv, fo_send)
-    c2.near()
+    stage("c2_far")
     c2.far()
-    forward([wop.at[c, heads]], fo_recv, fo_send)
+    forward([wop.at[c, heads, lax.rem(a_pos + 2, 4)]], fo_recv, fo_send)
     b2o.relay()
     stage("a2a_wait")
     l_re.wait()
-    for l in l_wp:
-        l.wait()
+    l_wp_all.wait()
     stage("wout")
 
     def project(j):
@@ -740,15 +749,13 @@
     b2o.far()
     b2.far()
     forward([wd.at[:, yf, c]], fw_dn2)
-    stage("up0")
-    up(0, None)
-    stage("down1_last")
-    dn_last.wait_recv()
-    first_sums(yf)
     stage("ag_far")
     ag.far()
     stage("up3")
     up(3, None)
+    stage("down1_last")
+    dn_last.wait_recv()
+    first_sums(yf)
     stage("down3")
     rs2, rs3 = [], []
     for i in range(2):
@@ -780,12 +787,18 @@
                 acc2[rows, lanes] + add_in[side, :, lanes].astype(F32)
             ).astype(BF16)
             rs3[2 * i + side].start()
+    stage("up0")
+    up(0, None)
     stage("down0")
     down(0, 0, 4, add_own)
     l_mx = cp.local(mixed, own_out)
     l_mx.start()
     stage("rs_wait")
     cp.waiter(rs_in, rs_send, rs_recv).wait_recv()
+    cp.drain_later(st_own, st_send, rs_recv)
+    cp.drain_later(q_recv, q_sends, rs_recv)
+    cp.drain_later(sc_recv, sc_sends, rs_recv)
+    cp.drain_later(ro, ro_send, rs_recv)
     l_mx.wait()
     stage("drain")
     assert (cp.sends, cp.recvs, cp.locals) == N_SEMS, (cp.sends, cp.recvs, cp.locals)

time: 101 us -> 100 us (0.990)
  no operation moved by 1% of the time
where the time goes in v5:
time: 100 us; the launch traced here: 99.1 us
  Pallas kernels  96 us (96%)
  other arithmetic  3.05 us (3%)
    pallas_call x1, Pallas kernels, shards(): pl.pallas_call(kernel, out_shape=(jax.ShapeDtypeStruct((ROWS, D), F32), j...  96 us
    convert_element_type x1, other arithmetic, shards(): return (own + sums[0].astype(F32) + sums[1].astype(F32)).astype(BF16)  3.05 us

profile of v5, /device:TPU:0, one launch (start us, length us, event | category | flops | bytes accessed | tf_op | source)
XLA Modules:
  0.0 99.1 jit_solution(3225128363089610641)
XLA Ops:
  0.0 96.0 %layer.1 = (f32[192,2048]{1,0:T(8,128)}, bf16[2,192,2048]{2,1,0:T(8,128)(2,1)}) custom-call(f32[2,1,768]{2,1,0:T(1,128)} %ig_h.1, f32[2,1,768]{2,1,0:T(1,128)} %fg_h.1, s32[768]{0:T(1024)} %doc_h.1, f32[1,512]{1,0:T(1,128)} %bitcast.13, f32[1,2048]{1,0:T(1,128)} %bitcast.12, bf16[768,256]{1,0:T(8,128)(2,1)} %q_h.1, bf16[768,256]{1,0:T(8,128)(2,1)} %k_h.1, ...), custom_call_target="tpu_custom_call" | custom-call | tf_op jit(solution)/shard_map/layer/pallas_call | solution.py:815
  96.0 3.0 %fusion = bf16[192,2048]{1,0:T(8,128)(2,1)} fusion(f32[192,2048]{1,0:T(8,128)} %get-tuple-element.7, bf16[2,192,2048]{2,1,0:T(8,128)(2,1)} %get-tuple-element.8), kind=kLoop, calls=%fused_computation.1 | loop fusion | flops 1966080 | bytes 3932160 | tf_op jit(solution)/shard_map/convert_element_type | solution.py:872

commit v6 on v5

--- a/solution.py
+++ b/solution.py
@@ -420,7 +420,6 @@
     stage("pieces")
     wp_all.wait_recv()
     c1.start()
-    b1.start1()
     stage("intra1")
     intra(256, 256)
     stage("intra2")
@@ -441,6 +440,7 @@
         rq[d].start()
         dq[d].start()
     stage("b1_relay")
+    b1.start1()
     b1.relay()
     stage("wr_relay")
     wr.relay()

time: 100 us -> 99.5 us (level)
  no operation moved by 1% of the time
where the time goes in v6:
time: 99.5 us; the launch traced here: 98.2 us
  Pallas kernels  95.1 us (96%)
  other arithmetic  3.05 us (3%)
    pallas_call x1, Pallas kernels, shards(): pl.pallas_call(kernel, out_shape=(jax.ShapeDtypeStruct((ROWS, D), F32), j...  95.1 us
    convert_element_type x1, other arithmetic, shards(): return (own + sums[0].astype(F32) + sums[1].astype(F32)).astype(BF16)  3.05 us

profile of v6, /device:TPU:0, one launch (start us, length us, event | category | flops | bytes accessed | tf_op | source)
XLA Modules:
  0.0 98.2 jit_solution(13561500508518996167)
XLA Ops:
  0.0 95.1 %layer.1 = (f32[192,2048]{1,0:T(8,128)}, bf16[2,192,2048]{2,1,0:T(8,128)(2,1)}) custom-call(f32[2,1,768]{2,1,0:T(1,128)} %ig_h.1, f32[2,1,768]{2,1,0:T(1,128)} %fg_h.1, s32[768]{0:T(1024)} %doc_h.1, f32[1,512]{1,0:T(1,128)} %bitcast.13, f32[1,2048]{1,0:T(1,128)} %bitcast.12, bf16[768,256]{1,0:T(8,128)(2,1)} %q_h.1, bf16[768,256]{1,0:T(8,128)(2,1)} %k_h.1, ...), custom_call_target="tpu_custom_call" | custom-call | tf_op jit(solution)/shard_map/layer/pallas_call | solution.py:815
  95.1 3.0 %fusion = bf16[192,2048]{1,0:T(8,128)(2,1)} fusion(f32[192,2048]{1,0:T(8,128)} %get-tuple-element.7, bf16[2,192,2048]{2,1,0:T(8,128)(2,1)} %get-tuple-element.8), kind=kLoop, calls=%fused_computation.1 | loop fusion | flops 1966080 | bytes 3932160 | tf_op jit(solution)/shard_map/convert_element_type | solution.py:872

commit v7 on v6

--- a/solution.py
+++ b/solution.py
@@ -564,12 +564,12 @@
             if step == 1:
                 second_phase()
     stage("a1_wait")
+    a1.near()
+    a1.far()
+    a2.start()
     b1.near()
     b1.far()
     b2.start()
-    a1.near()
-    a1.far()
-    a2.start()
     stage("a2a_relay")
     ca += [
         cp.remote(ro_st.at[0], ro.at[xm, lo], {"x": xp}, ro_send),

time: 99.5 us -> 99.5 us (level)
  no operation moved by 1% of the time
where the time goes in v7:
time: 99.5 us; the launch traced here: 98.2 us
  Pallas kernels  95.1 us (96%)
  other arithmetic  3.05 us (3%)
    pallas_call x1, Pallas kernels, shards(): pl.pallas_call(kernel, out_shape=(jax.ShapeDtypeStruct((ROWS, D), F32), j...  95.1 us
    convert_element_type x1, other arithmetic, shards(): return (own + sums[0].astype(F32) + sums[1].astype(F32)).astype(BF16)  3.05 us

profile of v7, /device:TPU:0, one launch (start us, length us, event | category | flops | bytes accessed | tf_op | source)
XLA Modules:
  0.0 98.2 jit_solution(8875766171391920065)
XLA Ops:
  0.0 95.1 %layer.1 = (f32[192,2048]{1,0:T(8,128)}, bf16[2,192,2048]{2,1,0:T(8,128)(2,1)}) custom-call(f32[2,1,768]{2,1,0:T(1,128)} %ig_h.1, f32[2,1,768]{2,1,0:T(1,128)} %fg_h.1, s32[768]{0:T(1024)} %doc_h.1, f32[1,512]{1,0:T(1,128)} %bitcast.13, f32[1,2048]{1,0:T(1,128)} %bitcast.12, bf16[768,256]{1,0:T(8,128)(2,1)} %q_h.1, bf16[768,256]{1,0:T(8,128)(2,1)} %k_h.1, ...), custom_call_target="tpu_custom_call" | custom-call | tf_op jit(solution)/shard_map/layer/pallas_call | solution.py:815
  95.1 3.0 %fusion = bf16[192,2048]{1,0:T(8,128)(2,1)} fusion(f32[192,2048]{1,0:T(8,128)} %get-tuple-element.7, bf16[2,192,2048]{2,1,0:T(8,128)(2,1)} %get-tuple-element.8), kind=kLoop, calls=%fused_computation.1 | loop fusion | flops 1966080 | bytes 3932160 | tf_op jit(solution)/shard_map/convert_element_type | solution.py:872
